TPU v7x, 32 devices: a whole 2x2x4 slice. The times are simulated.
32 devices in a mesh: grp: 2 (over y), fs: 4 (over z), tp: 4 (over x, core).
Axes of the slice: x: 2, y: 2, z: 4, core: 2. Of those that a mesh axis runs over, the one named last changes fastest.
Arguments:
- residual_in: bfloat16 [4096, 2048], P(('grp', 'fs', 'tp')), parts along dimension 0, may hold values from -6 to 6
- hidden_first: bfloat16 [4096, 5632], P(('grp', 'fs', 'tp')), parts along dimension 0, may hold values from -6 to 6
- down_weight: bfloat16 [5632, 2048], P('tp', 'fs'), may hold values from -0.078125 to 0.078125
- mixer_out: bfloat16 [4096, 2048], P(('grp', 'fs', 'tp')), parts along dimension 0, may hold values from -6 to 6
- norm_gain: float32 [2, 2048], replicated, may hold values from 0.1 to 1.9
- norm_shift: float32 [2, 2048], replicated, may hold values from -1.5 to 1.5
- gate_weight: bfloat16 [2048, 5632], P('fs', 'tp'), may hold values from -0.125 to 0.125
- up_weight: bfloat16 [2048, 5632], P('fs', 'tp'), may hold values from -0.125 to 0.125
Outputs:
- mixed_state: bfloat16 [4096, 2048], P(('grp', 'fs', 'tp')), parts along dimension 0
- hidden_second: bfloat16 [4096, 5632], P(('grp', 'fs'), 'tp'), parts along dimension 0
There are 2 independent parts, one for each index of `grp`. A program takes and returns all parts, laid end to end along the dimension named above; an argument that names none is the same for every part. Nothing has to cross between parts.
All inputs are finite; a program needn't handle non-finite values.
Results may differ from a plain program's by a relative error of at most 0.012.
Values may be sent and summed in bfloat16 or wider, within the bound.
A program may use at most 64 MiB of HBM per device.

v0:
```python
import functools

import jax
import jax.numpy as jnp
from jax import lax
from jax.experimental import pallas as pl
from jax.experimental.pallas import tpu as pltpu
from jax.sharding import PartitionSpec as P

MESH = pl.DeviceIdType.MESH


def layer_norm(values, gain, shift):
    center = values - jnp.mean(values, axis=-1, keepdims=True)
    variance = jnp.mean(center * center, axis=-1, keepdims=True)
    return center * lax.rsqrt(variance + 1e-05) * gain + shift


def kernel(
    sizes,
    res_ref,
    hid_ref,
    down_ref,
    mix_ref,
    gain_ref,
    shift_ref,
    gate_ref,
    up_ref,
    mixed_ref,
    out_ref,
    down_all,
    host_all,
    each_all,
    spread,
    part,
    red,
    mixed_all,
    host_acc,
    each_acc,
    back,
    load_sem,
    d_send,
    d_recv,
    h_send,
    h_recv,
    e_send,
    e_recv,
    a_send,
    a_recv,
    r_send,
    r_recv,
    m_send,
    m_recv,
    g_send,
    g_recv,
    b_send,
    b_recv,
):
    n_grp, n_fs, n_tp, sub = sizes
    shared = host_all.shape[3]
    g, f, t = lax.axis_index("grp"), lax.axis_index("fs"), lax.axis_index("tp")
    rows = res_ref.shape[0]
    width = gate_ref.shape[1]
    depth = gate_ref.shape[0]
    chunks = n_grp * sub

    def hid_block(peer):
        if len(hid_ref.shape) == 3:
            return hid_ref.at[peer]
        return hid_ref.at[:, pl.ds(pl.multiple_of(peer * width, width), width)]

    def own_rows(peer):
        return pl.ds(pl.multiple_of(peer * rows, rows), rows)

    load_down = pltpu.make_async_copy(down_ref, down_all.at[f], load_sem.at[0])
    loads = []
    for mat, ref in enumerate((gate_ref, up_ref)):
        loads.append(
            pltpu.make_async_copy(
                ref.at[:, pl.ds(0, shared)], host_all.at[f, mat], load_sem.at[1 + mat]
            )
        )
        loads.append(
            pltpu.make_async_copy(
                ref.at[:, pl.ds(shared, width - shared)], each_all.at[f, mat], load_sem.at[4 + mat]
            )
        )
    load_hid = pltpu.make_async_copy(hid_block(t), spread.at[own_rows(t)], load_sem.at[3])
    load_down.start()
    load_hid.start()
    for load in loads:
        load.start()

    lower = 2 * (f // 2)
    half = n_fs // 2
    host = lower + jnp.where(lower + 1 < half, 1, 0)
    is_host = f == host
    other = 2 * lower + 1 - f
    low_host = 1 if half > 1 else 0
    high_host = 2 * ((n_fs - 1) // 2)

    barrier = pltpu.get_barrier_semaphore()

    def greet(device):
        pl.semaphore_signal(barrier, inc=1, device_id=device, device_id_type=MESH)

    for d in range(1, n_grp):
        greet({"grp": lax.rem(g + d, n_grp)})
    for d in range(1, n_tp):
        greet({"tp": lax.rem(t + d, n_tp)})

    @pl.when(f > 0)
    def _():
        greet({"fs": f - 1})

    @pl.when(f < n_fs - 1)
    def _():
        greet({"fs": f + 1})

    inner = jnp.minimum(f, 1) + jnp.minimum(n_fs - 1 - f, 1)
    pl.semaphore_wait(barrier, n_grp - 1 + n_tp - 1 + inner)

    def block_copy(all_refs, send, recv):
        def copy(src, chunk, way, device):
            blocks = all_refs(src)
            size = blocks.shape[0] // chunks
            block = blocks.at[pl.ds(pl.multiple_of(chunk * size, size), size)]
            return pltpu.make_async_remote_copy(
                src_ref=block,
                dst_ref=block,
                send_sem=send(src).at[way, chunk],
                recv_sem=recv(src).at[chunk],
                device_id=device,
                device_id_type=MESH,
            )

        return copy

    def weight(refs, send, recv, mat):
        return block_copy(
            lambda src: refs.at[src, mat],
            lambda src: send.at[2 * src + mat],
            lambda src: recv.at[2 * src + mat],
        )

    def start(copy):
        copy.start()

    def wait_send(copy):
        copy.wait_send()

    class Gather:
        def __init__(self, copies, low, high, whole, needs):
            self.copies, self.low, self.high = copies, low, high
            self.whole, self.needs = whole, needs

        def whole_up(self, plane):
            return (2 * plane < n_fs) & self.whole

        def whole_down(self, plane):
            return (2 * plane >= n_fs) & self.whole

        def reached(self, plane):
            return (plane >= self.low) & (plane <= self.high)

        def along(self, copy, src, chunk, act, mine):
            up = (src <= f) & self.reached(f + 1)
            down = (src >= f) & self.reached(f - 1)
            if not mine:
                up = up & self.whole_up(f + 1)
                down = down & self.whole_down(f - 1)

            @pl.when(up)
            def _():
                act(copy(src, chunk, 0, {"fs": f + 1}))

            @pl.when(down)
            def _():
                act(copy(src, chunk, 1, {"fs": f - 1}))

        def all_along(self, src, act):
            for j in range(sub):
                for copy in self.copies:
                    self.along(copy, src, g * sub + j, act, True)
            if self.whole:
                for d in range(1, n_grp):
                    for j in range(sub):
                        for copy in self.copies:
                            chunk = lax.rem(g + d, n_grp) * sub + j
                            self.along(copy, src, chunk, act, False)

        def across(self, copy, src, chunk, act):
            for d in range(1, n_grp):
                act(copy(src, chunk, 1 + d, {"grp": lax.rem(g + d, n_grp)}))

        def whole_in(self, src):
            return ((src < f) & self.whole_up(f)) | ((src > f) & self.whole_down(f))

        def comes(self, src):
            return (src >= 0) & (src < n_fs) & (src != f) & self.reached(f)

        def swaps(self, src):
            return self.comes(src) & self.needs & jnp.logical_not(self.whole_in(src))

        def take(self, src):
            @pl.when(self.comes(src))
            def _():
                for j in range(sub):
                    for copy in self.copies:
                        chunk = g * sub + j
                        copy(src, chunk, 0, {"fs": other}).wait_recv()
                        self.along(copy, src, chunk, start, True)

                        @pl.when(self.swaps(src))
                        def _():
                            self.across(copy, src, chunk, start)

            if self.whole:

                @pl.when(self.comes(src) & self.whole_in(src))
                def _():
                    for d in range(1, n_grp):
                        for j in range(sub):
                            for copy in self.copies:
                                chunk = lax.rem(g + d, n_grp) * sub + j
                                copy(src, chunk, 0, {"fs": other}).wait_recv()
                                self.along(copy, src, chunk, start, False)

        def take_across(self, src):
            @pl.when(self.swaps(src))
            def _():
                for d in range(1, n_grp):
                    for j in range(sub):
                        for copy in self.copies:
                            chunk = lax.rem(g + d, n_grp) * sub + j
                            copy(src, chunk, 0, {"fs": other}).wait_recv()

        def drain(self, src):
            @pl.when((src == f) | self.comes(src))
            def _():
                if self.whole:
                    @pl.when((src == f) | self.whole_in(src))
                    def _():
                        for d in range(1, n_grp):
                            for j in range(sub):
                                for copy in self.copies:
                                    chunk = lax.rem(g + d, n_grp) * sub + j
                                    self.along(copy, src, chunk, wait_send, False)
                for j in range(sub):
                    for copy in self.copies:
                        self.along(copy, src, g * sub + j, wait_send, True)

            @pl.when(self.swaps(src))
            def _():
                for j in range(sub):
                    for copy in self.copies:
                        self.across(copy, src, g * sub + j, wait_send)

    def source(k):
        return f + (1 - 2 * lax.rem(k, 2)) * ((k + 1) // 2)

    def valid(src):
        return (src >= 0) & (src < n_fs)

    d_copy = block_copy(
        lambda src: down_all.at[src], lambda src: d_send.at[src], lambda src: d_recv.at[src]
    )
    down = Gather([d_copy], 0, n_fs - 1, False, True)
    hosted = Gather(
        [weight(host_all, h_send, h_recv, mat) for mat in range(2)],
        low_host,
        high_host,
        True,
        is_host,
    )
    each = Gather(
        [weight(each_all, e_send, e_recv, mat) for mat in range(2)], 0, n_fs - 1, True, True
    )

    def a_copy(d):
        peer = lax.rem(t + d, n_tp)
        return pltpu.make_async_remote_copy(
            src_ref=hid_block(peer),
            dst_ref=spread.at[own_rows(t)],
            send_sem=a_send.at[d],
            recv_sem=a_recv.at[d],
            device_id={"tp": peer},
            device_id_type=MESH,
        )

    def r_copy(src, d):
        peer = lax.rem(t + d, n_tp)
        return pltpu.make_async_remote_copy(
            src_ref=part.at[src, own_rows(peer)],
            dst_ref=red.at[d, src],
            send_sem=r_send.at[d, src],
            recv_sem=r_recv.at[d, src],
            device_id={"tp": peer},
            device_id_type=MESH,
        )

    core = lax.rem(t, 2)
    sibling = t + 1 - 2 * core

    def m_copy(owner, whose, hop):
        peer = sibling if hop == 0 else lax.rem(t + 2 * hop, n_tp)
        place = mixed_all.at[whose, own_rows(owner)]
        return pltpu.make_async_remote_copy(
            src_ref=place,
            dst_ref=place,
            send_sem=m_send.at[whose, owner, hop],
            recv_sem=m_recv.at[whose, owner],
            device_id={"tp": peer},
            device_id_type=MESH,
        )

    chips = n_tp // 2

    def m_out(whose):
        for hop in list(range(1, chips)) + [0]:
            m_copy(t, whose, hop).start()

    def m_relay(whose):
        for hop in range(1, chips):
            owner = lax.rem(t + 2 * hop, n_tp)
            m_copy(owner, whose, 0).wait_recv()
            m_copy(owner, whose, 0).start()

    def m_rest(whose):
        for hop in range(chips):
            m_copy(lax.rem(sibling + 2 * hop, n_tp), whose, 0).wait_recv()

    def m_drain(whose):
        for hop in range(chips):
            m_copy(t, whose, hop).wait_send()
        for hop in range(1, chips):
            m_copy(lax.rem(t + 2 * hop, n_tp), whose, 0).wait_send()

    def g_copy():
        return pltpu.make_async_remote_copy(
            src_ref=mixed_all.at[0, own_rows(t)],
            dst_ref=mixed_all.at[1, own_rows(t)],
            send_sem=g_send.at[0],
            recv_sem=g_recv.at[0],
            device_id={"fs": other},
            device_id_type=MESH,
        )

    tiles = 2
    tile = n_tp * rows // tiles

    def tile_rows(i):
        return pl.ds(pl.multiple_of(i * tile, tile), tile)

    def b_copy(i):
        return pltpu.make_async_remote_copy(
            src_ref=back.at[tile_rows(i)],
            dst_ref=out_ref.at[tile_rows(i), pl.ds(0, shared)],
            send_sem=b_send.at[i],
            recv_sem=b_recv.at[i],
            device_id={"fs": other},
            device_id_type=MESH,
        )

    load_down.wait()
    down.all_along(f, start)
    for d in range(1, n_tp):
        a_copy(d).start()
    for load in loads:
        load.wait()
    load_hid.wait()

    @pl.when(jnp.logical_not(is_host))
    def _():
        hosted.all_along(f, start)

    def first_half(k, carry):
        src = source(k)

        down.take(src)

        @pl.when((k == 2 * n_fs - 2) & is_host)
        def _():
            hosted.all_along(f, start)

        @pl.when(k == 2)
        def _():
            for d in range(1, n_tp):
                a_copy(d).wait_recv()

        done = source(k - 2)

        @pl.when((k >= 2) & valid(done))
        def _():
            down.take_across(done)
            part[done] = jnp.dot(
                spread[...], down_all[done], preferred_element_type=jnp.float32
            ).astype(jnp.bfloat16)
            for d in range(1, n_tp):
                r_copy(done, d).start()

        return carry

    lax.fori_loop(1, 2 * n_fs + 1, first_half, 0)

    for src in range(n_fs):
        for d in range(1, n_tp):
            r_copy(src, d).wait_recv()
    pieces = []
    for src in range(n_fs):
        total = part[src, own_rows(t)].astype(jnp.float32)
        for d in range(1, n_tp):
            total = total + red[d, src].astype(jnp.float32)
        pieces.append(total)
    branch = jnp.concatenate(pieces, axis=1)
    first = layer_norm(
        jnp.sqrt(2.0) * res_ref[...].astype(jnp.float32) + 0.5 * branch,
        gain_ref[0:1],
        shift_ref[0:1],
    )
    mixed = layer_norm(
        jnp.sqrt(2.0) * first + mix_ref[...].astype(jnp.float32), gain_ref[1:2], shift_ref[1:2]
    ).astype(jnp.bfloat16)
    mixed_all[0, own_rows(t)] = mixed
    mixed_ref[...] = mixed

    @pl.when(jnp.logical_not(is_host))
    def _():
        g_copy().start()

    m_out(0)

    @pl.when(jnp.logical_not(is_host))
    def _():
        each.all_along(f, start)

    def take_hosted(k, carry):
        hosted.take(source(k))
        return carry

    lax.fori_loop(1, 2 * n_fs - 1, take_hosted, 0)

    @pl.when(is_host)
    def _():
        each.all_along(f, start)

    m_relay(0)

    @pl.when(is_host)
    def _():
        g_copy().wait_recv()
        m_out(1)

    def take_each(k, carry):
        each.take(source(k))
        return carry

    lax.fori_loop(1, 3, take_each, 0)
    m_rest(0)

    def products(whose, span, gather, refs, total):
        total[...] = jnp.zeros_like(total)

        def add(k, carry):
            src = source(k)

            @pl.when(valid(src))
            def _():
                if gather is not None:
                    gather.take_across(src)
                here = pl.ds(pl.multiple_of(src * depth, depth), depth)
                for mat in range(2):
                    total[mat] += jnp.dot(
                        mixed_all[whose, span, here],
                        refs[src, mat],
                        preferred_element_type=jnp.float32,
                    )

            return carry

        lax.fori_loop(0, 2 * n_fs - 1, add, 0)
        gate = total[0]
        return (gate / (1.0 + jnp.exp(-gate)) * total[1]).astype(jnp.bfloat16)

    everything = pl.ds(0, n_tp * rows)

    @pl.when(is_host)
    def _():
        m_relay(1)
        out_ref[:, pl.ds(0, shared)] = products(0, everything, hosted, host_all, host_acc)

    lax.fori_loop(3, 2 * n_fs - 1, take_each, 0)

    @pl.when(is_host)
    def _():
        m_rest(1)

        def serve(i, carry):
            back[tile_rows(i)] = products(
                1, tile_rows(i), None, host_all, host_acc.at[:, pl.ds(0, tile)]
            )
            b_copy(i).start()
            return carry

        lax.fori_loop(0, tiles, serve, 0)

    out_ref[:, pl.ds(shared, width - shared)] = products(0, everything, each, each_all, each_acc)

    @pl.when(is_host)
    def _():
        for i in range(tiles):
            b_copy(i).wait_send()
        m_drain(1)

    @pl.when(jnp.logical_not(is_host))
    def _():
        g_copy().wait_send()
        for i in range(tiles):
            b_copy(i).wait_recv()

    m_drain(0)
    for d in range(1, n_tp):
        a_copy(d).wait_send()
        for src in range(n_fs):
            r_copy(src, d).wait_send()

    def drain(src, carry):
        for gather in (down, hosted, each):
            gather.drain(src)
        return carry

    lax.fori_loop(0, n_fs, drain, 0)


def on_device(
    sizes,
    residual_in,
    hidden_first,
    down_weight,
    mixer_out,
    norm_gain,
    norm_shift,
    gate_weight,
    up_weight,
):
    n_grp, n_fs, n_tp = sizes
    rows, model = residual_in.shape
    depth, width = gate_weight.shape
    cols = down_weight.shape[1]
    sub = 1
    if depth % (n_grp * 2 * 32) == 0 and down_weight.shape[0] % (n_grp * 2 * 32) == 0:
        sub = 2
    chunks = n_grp * sub
    each = max(1, width * 3 // (11 * 128)) * 128
    shared = (width - each) // 128 * 128
    each = width - shared
    if width % 128:
        hidden_first = hidden_first.reshape(rows, n_tp, width).transpose(1, 0, 2)
    vmem = pl.BlockSpec(memory_space=pltpu.VMEM)
    anywhere = pl.BlockSpec(memory_space=pl.ANY)
    dma = pltpu.SemaphoreType.DMA
    tokens = rows * n_tp
    return pl.pallas_call(
        functools.partial(kernel, (n_grp, n_fs, n_tp, sub)),
        out_shape=(
            jax.ShapeDtypeStruct((rows, model), jnp.bfloat16),
            jax.ShapeDtypeStruct((tokens, width), jnp.bfloat16),
        ),
        in_specs=[vmem, anywhere, anywhere, vmem, vmem, vmem, anywhere, anywhere],
        out_specs=(vmem, vmem),
        scratch_shapes=[
            pltpu.VMEM((n_fs,) + down_weight.shape, jnp.bfloat16),
            pltpu.VMEM((n_fs, 2, depth, shared), jnp.bfloat16),
            pltpu.VMEM((n_fs, 2, depth, each), jnp.bfloat16),
            pltpu.VMEM((tokens, width), jnp.bfloat16),
            pltpu.VMEM((n_fs, tokens, cols), jnp.bfloat16),
            pltpu.VMEM((n_tp, n_fs, rows, cols), jnp.bfloat16),
            pltpu.VMEM((2, tokens, model), jnp.bfloat16),
            pltpu.VMEM((2, tokens, shared), jnp.float32),
            pltpu.VMEM((2, tokens, each), jnp.float32),
            pltpu.VMEM((tokens, shared), jnp.bfloat16),
            dma((6,)),
            dma((n_fs, 1 + n_grp, chunks)),
            dma((n_fs, chunks)),
            dma((2 * n_fs, 1 + n_grp, chunks)),
            dma((2 * n_fs, chunks)),
            dma((2 * n_fs, 1 + n_grp, chunks)),
            dma((2 * n_fs, chunks)),
            dma((n_tp,)),
            dma((n_tp,)),
            dma((n_tp, n_fs)),
            dma((n_tp, n_fs)),
            dma((2, n_tp, n_tp // 2)),
            dma((2, n_tp)),
            dma((1,)),
            dma((1,)),
            dma((2,)),
            dma((2,)),
        ],
        compiler_params=pltpu.CompilerParams(
            collective_id=0, has_side_effects=True, vmem_limit_bytes=60 * 1024 * 1024
        ),
        name="half_steps",
    )(
        residual_in,
        hidden_first,
        down_weight,
        mixer_out,
        norm_gain,
        norm_shift,
        gate_weight,
        up_weight,
    )


def solution(mesh):
    sizes = tuple(mesh.shape[axis] for axis in ("grp", "fs", "tp"))
    in_specs = (
        P(("grp", "fs", "tp"), None),
        P(("grp", "fs", "tp"), None),
        P("tp", "fs"),
        P(("grp", "fs", "tp"), None),
        P(),
        P(),
        P("fs", "tp"),
        P("fs", "tp"),
    )
    out_specs = (P(("grp", "fs", "tp"), None), P(("grp", "fs"), "tp"))
    return jax.shard_map(
        functools.partial(on_device, sizes),
        mesh=mesh,
        in_specs=in_specs,
        out_specs=out_specs,
        check_vma=False,
    )
```

profile of v0, /device:TPU:0, one launch (start us, length us, event | category | flops | bytes accessed | tf_op | source)
XLA Modules:
  0.0 166.2 jit_solution(10090212373627282068)
XLA Ops:
  0.6 161.1 %half_steps.1 = (bf16[128,2048]{1,0:T(8,128)(2,1)}, bf16[512,1408]{1,0:T(8,128)(2,1)}) custom-call(bf16[128,2048]{1,0:T(8,128)(2,1)} %res_ref.1, bf16[128,5632]{1,0:T(8,128)(2,1)} %hid_ref.1, bf16[1408,512]{1,0:T(8,128)(2,1)} %down_ref.1, bf16[128,2048]{1,0:T(8,128)(2,1)} %mix_ref.1, f32[2,2048]{1,0:T(2,128)} %gain_ref.1, f32[2,2048]{1,0:T(2,128)} %shift_ref.1, ...), custom_call_target="tpu_custom_call" | custom-call | tf_op jit(solution)/shard_map/half_steps/pallas_call | solution.py:563
  161.8 1.9 %copy.12 = bf16[128,2048]{1,0:T(8,128)(2,1)} copy(bf16[128,2048]{1,0:T(8,128)(2,1)} %get-tuple-element.4) | data formatting | bytes 1048576
  163.7 2.6 %copy.13 = bf16[512,1408]{1,0:T(8,128)(2,1)} copy(bf16[512,1408]{1,0:T(8,128)(2,1)} %get-tuple-element.5) | data formatting | bytes 2883584
where the time goes:
time: 166 us
  Pallas kernels  161 us (97%)
  local copies, waits for them, and re-layouts  4.45 us (3%)
    pallas_call x1, Pallas kernels, on_device(): pl.pallas_call(functools.partial(kernel, (n_grp, n_fs, n_tp, sub)), out_s...  161 us
    unnamed x2, local copies, waits for them, and re-layouts  4.45 us

commit v1 on v0

--- a/solution.py
+++ b/solution.py
@@ -532,6 +532,600 @@
     lax.fori_loop(0, n_fs, drain, 0)
 
 
+def paired_kernel(
+    sizes,
+    res_ref,
+    hid_ref,
+    down_ref,
+    mix_ref,
+    gain_ref,
+    shift_ref,
+    gate_ref,
+    up_ref,
+    mixed_ref,
+    out_ref,
+    down_all,
+    cols_all,
+    spread,
+    part,
+    red,
+    mixed_all,
+    back,
+    load_sem,
+    c_load,
+    d_send,
+    d_recv,
+    c_send,
+    c_recv,
+    a_send,
+    a_recv,
+    r_send,
+    r_recv,
+    m_send,
+    m_recv,
+    g_send,
+    g_recv,
+    b_send,
+    b_recv,
+):
+    n_grp, n_fs, n_tp, sub, own, moved, pieces = sizes
+    g, f, t = lax.axis_index("grp"), lax.axis_index("fs"), lax.axis_index("tp")
+    rows = res_ref.shape[0]
+    width = gate_ref.shape[1]
+    depth = gate_ref.shape[0]
+    n_col = cols_all.shape[0]
+    lanes = width // n_col
+
+    lower = 2 * (f // 2)
+    mate = 2 * lower + 1 - f
+    inner = (f > 0) & (f < n_fs - 1)
+    outer = jnp.logical_not(inner)
+    facing = n_fs - 1 - jnp.where(inner, f, mate)
+    beyond = n_fs - 1 - jnp.where(inner, mate, f)
+
+    def hid_block(peer):
+        return hid_ref.at[:, pl.ds(pl.multiple_of(peer * width, width), width)]
+
+    def own_rows(peer):
+        return pl.ds(pl.multiple_of(peer * rows, rows), rows)
+
+    load_down = pltpu.make_async_copy(down_ref, down_all.at[f], load_sem.at[0])
+    load_hid = pltpu.make_async_copy(hid_block(t), spread.at[own_rows(t)], load_sem.at[1])
+
+    def load_col(c, mat):
+        return pltpu.make_async_copy(
+            (gate_ref, up_ref)[mat].at[:, pl.ds(pl.multiple_of(c * lanes, lanes), lanes)],
+            cols_all.at[c, f, :, pl.ds(mat * lanes, lanes)],
+            c_load.at[c, mat],
+        )
+
+    load_down.start()
+    load_hid.start()
+
+    def each_col(low, high, act):
+        def body(c, carry):
+            act(c)
+            return carry
+
+        lax.fori_loop(low, high, body, 0)
+
+    def load_cols(c):
+        for mat in range(2):
+            load_col(c, mat).start()
+
+    def loaded_cols(c):
+        for mat in range(2):
+            load_col(c, mat).wait()
+
+    each_col(0, n_col, load_cols)
+
+    barrier = pltpu.get_barrier_semaphore()
+
+    def greet(device):
+        pl.semaphore_signal(barrier, inc=1, device_id=device, device_id_type=MESH)
+
+    for d in range(1, n_grp):
+        greet({"grp": lax.rem(g + d, n_grp)})
+    for d in range(1, n_tp):
+        greet({"tp": lax.rem(t + d, n_tp)})
+    greet({"fs": mate})
+
+    @pl.when(inner)
+    def _():
+        greet({"fs": facing})
+
+    pl.semaphore_wait(barrier, n_grp - 1 + n_tp - 1 + 1 + inner.astype(jnp.int32))
+
+    MAIN, OUT, ACROSS = 0, 1, 2
+
+    def device_of(way):
+        if way == MAIN:
+            return {"fs": jnp.where(inner, facing, mate)}
+        if way == OUT:
+            return {"fs": mate}
+        return {"grp": lax.rem(g + way - ACROSS + 1, n_grp)}
+
+    def d_copy(src, share, j, way):
+        size = down_all.shape[1] // (n_grp * sub)
+        place = share * sub + j
+        block = down_all.at[src, pl.ds(pl.multiple_of(place * size, size), size)]
+        return pltpu.make_async_remote_copy(
+            src_ref=block,
+            dst_ref=block,
+            send_sem=d_send.at[way, src, place],
+            recv_sem=d_recv.at[src, place],
+            device_id=device_of(way),
+            device_id_type=MESH,
+        )
+
+    def c_copy(c, src, share, way):
+        size = depth // n_grp
+        block = cols_all.at[c, src, pl.ds(pl.multiple_of(share * size, size), size)]
+        return pltpu.make_async_remote_copy(
+            src_ref=block,
+            dst_ref=block,
+            send_sem=c_send.at[way, src, c, share],
+            recv_sem=c_recv.at[src, c, share],
+            device_id=device_of(way),
+            device_id_type=MESH,
+        )
+
+    across = [ACROSS + d - 1 for d in range(1, n_grp)]
+    others = [lax.rem(g + d, n_grp) for d in range(1, n_grp)]
+
+    def d_send_on(src, share, j, ways):
+        for way in ways:
+            d_copy(src, share, j, way).start()
+
+    def c_send_on(c, src, share, ways):
+        for way in ways:
+            c_copy(c, src, share, way).start()
+
+    def d_pass(src, j, ways):
+        d_copy(src, g, j, MAIN).wait_recv()
+        d_send_on(src, g, j, ways)
+
+    def c_pass(c, src, ways):
+        c_copy(c, src, g, MAIN).wait_recv()
+        c_send_on(c, src, g, ways)
+
+    def d_rest(src):
+        for share in others:
+            for j in range(sub):
+                d_copy(src, share, j, MAIN).wait_recv()
+
+    def c_rest(c, src):
+        for share in others:
+            c_copy(c, src, share, MAIN).wait_recv()
+
+    def a_copy(d):
+        peer = lax.rem(t + d, n_tp)
+        return pltpu.make_async_remote_copy(
+            src_ref=hid_block(peer),
+            dst_ref=spread.at[own_rows(t)],
+            send_sem=a_send.at[d],
+            recv_sem=a_recv.at[d],
+            device_id={"tp": peer},
+            device_id_type=MESH,
+        )
+
+    def r_copy(src, d):
+        peer = lax.rem(t + d, n_tp)
+        return pltpu.make_async_remote_copy(
+            src_ref=part.at[src, own_rows(peer)],
+            dst_ref=red.at[d, src],
+            send_sem=r_send.at[d, src],
+            recv_sem=r_recv.at[d, src],
+            device_id={"tp": peer},
+            device_id_type=MESH,
+        )
+
+    core = lax.rem(t, 2)
+    sibling = t + 1 - 2 * core
+    chips = n_tp // 2
+    piece = rows // pieces
+
+    def piece_rows(owner, q):
+        return pl.ds(pl.multiple_of(owner * rows + q * piece, piece), piece)
+
+    def m_copy(owner, whose, hop, q):
+        peer = sibling if hop == 0 else lax.rem(t + 2 * hop, n_tp)
+        place = mixed_all.at[whose, piece_rows(owner, q)]
+        return pltpu.make_async_remote_copy(
+            src_ref=place,
+            dst_ref=place,
+            send_sem=m_send.at[whose, owner, hop, q],
+            recv_sem=m_recv.at[whose, owner, q],
+            device_id={"tp": peer},
+            device_id_type=MESH,
+        )
+
+    def m_out(whose, q):
+        for hop in list(range(1, chips)) + [0]:
+            m_copy(t, whose, hop, q).start()
+
+    def m_relay(whose, q):
+        for hop in range(1, chips):
+            owner = lax.rem(t + 2 * hop, n_tp)
+            m_copy(owner, whose, 0, q).wait_recv()
+            m_copy(owner, whose, 0, q).start()
+
+    def m_rest(whose, q):
+        for hop in range(chips):
+            m_copy(lax.rem(sibling + 2 * hop, n_tp), whose, 0, q).wait_recv()
+
+    def m_drain(whose, q):
+        for hop in range(chips):
+            m_copy(t, whose, hop, q).wait_send()
+        for hop in range(1, chips):
+            m_copy(lax.rem(t + 2 * hop, n_tp), whose, 0, q).wait_send()
+
+    def g_copy(q):
+        return pltpu.make_async_remote_copy(
+            src_ref=mixed_all.at[0, piece_rows(t, q)],
+            dst_ref=mixed_all.at[1, piece_rows(t, q)],
+            send_sem=g_send.at[q],
+            recv_sem=g_recv.at[q],
+            device_id={"fs": mate},
+            device_id_type=MESH,
+        )
+
+    def col_lanes(c):
+        return pl.ds(pl.multiple_of(c * lanes, lanes), lanes)
+
+    def b_copy(c):
+        return pltpu.make_async_remote_copy(
+            src_ref=back.at[c - own],
+            dst_ref=out_ref.at[:, col_lanes(c)],
+            send_sem=b_send.at[c - own],
+            recv_sem=b_recv.at[c - own],
+            device_id={"fs": mate},
+            device_id_type=MESH,
+        )
+
+    def first_product(src):
+        part[src] = jnp.dot(
+            spread[...], down_all[src], preferred_element_type=jnp.float32
+        ).astype(jnp.bfloat16)
+        for d in range(1, n_tp):
+            r_copy(src, d).start()
+
+    def take_hidden():
+        load_hid.wait()
+        for d in range(1, n_tp):
+            a_copy(d).wait_recv()
+
+    def norms():
+        for src in range(n_fs):
+            for d in range(1, n_tp):
+                r_copy(src, d).wait_recv()
+        columns = []
+        for src in range(n_fs):
+            total = part[src, own_rows(t)].astype(jnp.float32)
+            for d in range(1, n_tp):
+                total = total + red[d, src].astype(jnp.float32)
+            columns.append(total)
+        branch = jnp.concatenate(columns, axis=1)
+        first = layer_norm(
+            jnp.sqrt(2.0) * res_ref[...].astype(jnp.float32) + 0.5 * branch,
+            gain_ref[0:1],
+            shift_ref[0:1],
+        )
+        mixed = layer_norm(
+            jnp.sqrt(2.0) * first + mix_ref[...].astype(jnp.float32),
+            gain_ref[1:2],
+            shift_ref[1:2],
+        ).astype(jnp.bfloat16)
+        mixed_all[0, own_rows(t)] = mixed
+        mixed_ref[...] = mixed
+
+    def second_product(whose, c):
+        weight = cols_all[c].reshape(n_fs * depth, 2 * lanes)
+        total = jnp.dot(mixed_all[whose], weight, preferred_element_type=jnp.float32)
+        gate = total[:, :lanes]
+        return (gate / (1.0 + jnp.exp(-gate)) * total[:, lanes:]).astype(jnp.bfloat16)
+
+    load_down.wait()
+
+    @pl.when(inner)
+    def _():
+        for j in range(sub):
+            d_send_on(f, g, j, (MAIN, OUT))
+
+    @pl.when(outer)
+    def _():
+        for share in [g] + others:
+            for j in range(sub):
+                d_send_on(f, share, j, (MAIN,))
+
+    for d in range(1, n_tp):
+        a_copy(d).start()
+    each_col(0, n_col, loaded_cols)
+
+    @pl.when(outer)
+    def _():
+        each_col(0, n_col, lambda c: c_send_on(c, f, g, (MAIN,)))
+
+    ahead = min(4, n_col)
+    early = min(2, n_col)
+
+    @pl.when(inner)
+    def _():
+        for j in range(sub):
+            d_pass(mate, j, (MAIN,))
+            d_pass(facing, j, [OUT] + across)
+        for c in range(ahead):
+            c_send_on(c, f, g, (MAIN,))
+
+    @pl.when(outer)
+    def _():
+        for j in range(sub):
+            d_pass(mate, j, across)
+
+    take_hidden()
+
+    def step(k, carry):
+        @pl.when((k == 1) & inner)
+        def _():
+            for j in range(sub):
+                d_pass(beyond, j, [OUT] + across)
+            each_col(0, own, lambda c: c_send_on(c, f, g, (OUT,)))
+            d_rest(mate)
+
+        @pl.when((k == 1) & outer)
+        def _():
+            for j in range(sub):
+                d_pass(facing, j, across)
+            d_rest(mate)
+
+        @pl.when((k == 2) & outer)
+        def _():
+            for j in range(sub):
+                d_pass(beyond, j, across)
+
+        @pl.when(k == 2)
+        def _():
+            d_rest(facing)
+
+        @pl.when((k >= 2) & (k - 2 < early) & inner)
+        def _():
+            c_pass(k - 2, mate, (MAIN,))
+
+        @pl.when(k == 3)
+        def _():
+            d_rest(beyond)
+
+        first_product(
+            jnp.where(k == 0, f, jnp.where(k == 1, mate, jnp.where(k == 2, facing, beyond)))
+        )
+        return carry
+
+    lax.fori_loop(0, n_fs, step, 0)
+    norms()
+
+    def swapped(c):
+        return c >= n_col - moved
+
+    def serve(c):
+        c_rest(c, mate)
+        c_rest(c, facing)
+        c_rest(c, beyond)
+        out_ref[:, col_lanes(c)] = second_product(0, c)
+
+        @pl.when(c >= own)
+        def _():
+            back[c - own] = second_product(1, c)
+            b_copy(c).start()
+
+    def relay(c):
+        @pl.when(c >= early)
+        def _():
+            c_pass(c, mate, (MAIN,))
+
+        @pl.when(swapped(c))
+        def _():
+            c_send_on(c, mate, g, across)
+
+        @pl.when(c + ahead < n_col)
+        def _():
+            c_send_on(c + ahead, f, g, (MAIN,))
+
+        for src in (facing, beyond):
+            c_pass(c, src, across)
+
+            @pl.when(c < own)
+            def _():
+                c_send_on(c, src, g, (OUT,))
+
+    def relay_and_serve(c):
+        relay(c)
+        first = c - (n_col - 4)
+
+        def from_mate(q):
+            g_copy(q).wait_recv()
+            m_out(1, q)
+
+        @pl.when(c == n_col - 8)
+        def _():
+            for q in range(pieces):
+                m_relay(0, q)
+
+        @pl.when(c == n_col - 5)
+        def _():
+            for q in range(pieces // 2):
+                from_mate(q)
+            for q in range(pieces):
+                m_rest(0, q)
+
+        @pl.when(c == n_col - 4)
+        def _():
+            for q in range(pieces // 2, pieces):
+                from_mate(q)
+            for q in range(pieces // 2):
+                m_relay(1, q)
+
+        @pl.when(c == n_col - 3)
+        def _():
+            for q in range(pieces // 2, pieces):
+                m_relay(1, q)
+            for q in range(pieces):
+                m_rest(1, q)
+
+        low = jnp.where(first < 1, 0, 2 * (first - 1))
+        high = jnp.where(first < 1, 0, jnp.where(c == n_col - 1, n_col, 2 * first))
+        each_col(low, high, serve)
+
+    @pl.when(inner)
+    def _():
+        for q in range(pieces):
+            m_out(0, q)
+        each_col(0, n_col, relay_and_serve)
+
+    @pl.when(outer)
+    def _():
+        for q in range(pieces):
+            g_copy(q).start()
+            m_out(0, q)
+        for share in others:
+            each_col(0, n_col - moved, lambda c: c_send_on(c, f, share, (MAIN,)))
+
+        def pass_own(c):
+            for src in (mate, facing, beyond):
+                c_pass(c, src, across)
+
+        each_col(0, own, pass_own)
+        for q in range(pieces):
+            m_relay(0, q)
+        for q in range(pieces):
+            m_rest(0, q)
+
+        def make_own(c):
+            for src in (mate, facing, beyond):
+                c_rest(c, src)
+            out_ref[:, col_lanes(c)] = second_product(0, c)
+
+        each_col(0, own, make_own)
+        each_col(own, n_col, lambda c: b_copy(c).wait_recv())
+
+    for d in range(1, n_tp):
+        a_copy(d).wait_send()
+        for src in range(n_fs):
+            r_copy(src, d).wait_send()
+    for q in range(pieces):
+        m_drain(0, q)
+
+    def d_sent(src, share, ways):
+        for j in range(sub):
+            for way in ways:
+                d_copy(src, share, j, way).wait_send()
+
+    def c_sent(low, high, src, share, ways):
+        def act(c):
+            for way in ways:
+                c_copy(c, src, share, way).wait_send()
+
+        each_col(low, high, act)
+
+    @pl.when(inner)
+    def _():
+        d_sent(f, g, (MAIN, OUT))
+        d_sent(mate, g, (MAIN,))
+        c_sent(0, n_col, f, g, (MAIN,))
+        c_sent(0, n_col, mate, g, (MAIN,))
+        c_sent(0, own, f, g, (OUT,))
+        c_sent(n_col - moved, n_col, mate, g, across)
+        for src in (facing, beyond):
+            d_sent(src, g, [OUT] + across)
+            c_sent(0, n_col, src, g, across)
+            c_sent(0, own, src, g, (OUT,))
+        for q in range(pieces):
+            m_drain(1, q)
+        each_col(own, n_col, lambda c: b_copy(c).wait_send())
+
+    @pl.when(outer)
+    def _():
+        for share in [g] + others:
+            d_sent(f, share, (MAIN,))
+        c_sent(0, n_col, f, g, (MAIN,))
+        for share in others:
+            c_sent(0, n_col - moved, f, share, (MAIN,))
+        for src in (mate, facing, beyond):
+            d_sent(src, g, across)
+            c_sent(0, own, src, g, across)
+        for q in range(pieces):
+            g_copy(q).wait_send()
+
+
+def paired_call(sizes, arguments):
+    n_grp, n_fs, n_tp = sizes
+    residual_in, hidden_first, down_weight, _, _, _, gate_weight, _ = arguments
+    rows, model = residual_in.shape
+    depth, width = gate_weight.shape
+    cols = down_weight.shape[1]
+    tokens = rows * n_tp
+    lanes = 128
+    n_col = width // lanes
+    sub = 4
+    own = max(1, n_col * 4 // 11)
+    moved = 1
+    pieces = 4
+    vmem = pl.BlockSpec(memory_space=pltpu.VMEM)
+    anywhere = pl.BlockSpec(memory_space=pl.ANY)
+    dma = pltpu.SemaphoreType.DMA
+    return pl.pallas_call(
+        functools.partial(paired_kernel, (n_grp, n_fs, n_tp, sub, own, moved, pieces)),
+        out_shape=(
+            jax.ShapeDtypeStruct((rows, model), jnp.bfloat16),
+            jax.ShapeDtypeStruct((tokens, width), jnp.bfloat16),
+        ),
+        in_specs=[vmem, anywhere, anywhere, vmem, vmem, vmem, anywhere, anywhere],
+        out_specs=(vmem, vmem),
+        scratch_shapes=[
+            pltpu.VMEM((n_fs,) + down_weight.shape, jnp.bfloat16),
+            pltpu.VMEM((n_col, n_fs, depth, 2 * lanes), jnp.bfloat16),
+            pltpu.VMEM((tokens, width), jnp.bfloat16),
+            pltpu.VMEM((n_fs, tokens, cols), jnp.bfloat16),
+            pltpu.VMEM((n_tp, n_fs, rows, cols), jnp.bfloat16),
+            pltpu.VMEM((2, tokens, model), jnp.bfloat16),
+            pltpu.VMEM((n_col - own, tokens, lanes), jnp.bfloat16),
+            dma((2,)),
+            dma((n_col, 2)),
+            dma((1 + n_grp, n_fs, n_grp * sub)),
+            dma((n_fs, n_grp * sub)),
+            dma((1 + n_grp, n_fs, n_col, n_grp)),
+            dma((n_fs, n_col, n_grp)),
+            dma((n_tp,)),
+            dma((n_tp,)),
+            dma((n_tp, n_fs)),
+            dma((n_tp, n_fs)),
+            dma((2, n_tp, n_tp // 2, pieces)),
+            dma((2, n_tp, pieces)),
+            dma((pieces,)),
+            dma((pieces,)),
+            dma((n_col - own,)),
+            dma((n_col - own,)),
+        ],
+        compiler_params=pltpu.CompilerParams(
+            collective_id=0, has_side_effects=True, vmem_limit_bytes=60 * 1024 * 1024
+        ),
+        name="paired_half_steps",
+    )(*arguments)
+
+
+def fits_pairs(sizes, residual_in, down_weight, gate_weight):
+    n_grp, n_fs, n_tp = sizes
+    depth, width = gate_weight.shape
+    return (
+        n_fs == 4
+        and n_tp % 2 == 0
+        and width % 128 == 0
+        and width // 128 >= 9
+        and depth % (n_grp * 32) == 0
+        and down_weight.shape[0] % (n_grp * 4 * 16) == 0
+        and residual_in.shape[0] % (4 * 16) == 0
+    )
+
+
 def on_device(
     sizes,
     residual_in,
@@ -543,6 +1137,18 @@
     gate_weight,
     up_weight,
 ):
+    if fits_pairs(sizes, residual_in, down_weight, gate_weight):
+        arguments = (
+            residual_in,
+            hidden_first,
+            down_weight,
+            mixer_out,
+            norm_gain,
+            norm_shift,
+            gate_weight,
+            up_weight,
+        )
+        return paired_call(sizes, arguments)
     n_grp, n_fs, n_tp = sizes
     rows, model = residual_in.shape
     depth, width = gate_weight.shape

time: 166 us -> 152 us (0.916)
  Pallas kernels: 161 us -> 147 us
    pallas_call x1, Pallas kernels: 161 us -> 147 us  [paired_call(): pl.pallas_call(functools.partial(paired_kernel, (n_grp, n_fs, n_tp, sub,...]
where the time goes in v1:
time: 152 us
  Pallas kernels  147 us (97%)
  local copies, waits for them, and re-layouts  4.45 us (3%)
    pallas_call x1, Pallas kernels, paired_call(): pl.pallas_call(functools.partial(paired_kernel, (n_grp, n_fs, n_tp, sub,...  147 us
    unnamed x2, local copies, waits for them, and re-layouts  4.45 us

profile of v1, /device:TPU:0, one launch (start us, length us, event | category | flops | bytes accessed | tf_op | source)
XLA Modules:
  0.0 152.1 jit_solution(505717501148455376)
XLA Ops:
  0.6 147.0 %paired_half_steps.1 = (bf16[128,2048]{1,0:T(8,128)(2,1)}, bf16[512,1408]{1,0:T(8,128)(2,1)}) custom-call(bf16[128,2048]{1,0:T(8,128)(2,1)} %res_ref.1, bf16[128,5632]{1,0:T(8,128)(2,1)} %hid_ref.1, bf16[1408,512]{1,0:T(8,128)(2,1)} %down_ref.1, bf16[128,2048]{1,0:T(8,128)(2,1)} %mix_ref.1, f32[2,2048]{1,0:T(2,128)} %gain_ref.1, f32[2,2048]{1,0:T(2,128)} %shift_ref.1, ...), custom_call_target="tpu_custom_call" | custom-call | tf_op jit(solution)/shard_map/paired_half_steps/pallas_call | solution.py:1075
  147.7 1.9 %copy.12 = bf16[128,2048]{1,0:T(8,128)(2,1)} copy(bf16[128,2048]{1,0:T(8,128)(2,1)} %get-tuple-element.4) | data formatting | bytes 1048576
  149.5 2.6 %copy.13 = bf16[512,1408]{1,0:T(8,128)(2,1)} copy(bf16[512,1408]{1,0:T(8,128)(2,1)} %get-tuple-element.5) | data formatting | bytes 2883584

commit v2 on v1

--- a/solution.py
+++ b/solution.py
@@ -551,24 +551,26 @@
     red,
     mixed_all,
     back,
+    result,
     load_sem,
-    c_load,
     d_send,
     d_recv,
+    d_late,
     c_send,
     c_recv,
-    a_send,
-    a_recv,
-    r_send,
-    r_recv,
+    c_late,
+    a_sem,
+    r_sem,
     m_send,
     m_recv,
+    m_late,
     g_send,
     g_recv,
     b_send,
     b_recv,
+    w_sem,
 ):
-    n_grp, n_fs, n_tp, sub, own, moved, pieces = sizes
+    n_grp, n_fs, n_tp, sub, own, pieces = sizes
     g, f, t = lax.axis_index("grp"), lax.axis_index("fs"), lax.axis_index("tp")
     rows = res_ref.shape[0]
     width = gate_ref.shape[1]
@@ -596,13 +598,13 @@
         return pltpu.make_async_copy(
             (gate_ref, up_ref)[mat].at[:, pl.ds(pl.multiple_of(c * lanes, lanes), lanes)],
             cols_all.at[c, f, :, pl.ds(mat * lanes, lanes)],
-            c_load.at[c, mat],
+            load_sem.at[2],
         )
 
     load_down.start()
     load_hid.start()
 
-    def each_col(low, high, act):
+    def each(low, high, act):
         def body(c, carry):
             act(c)
             return carry
@@ -613,11 +615,10 @@
         for mat in range(2):
             load_col(c, mat).start()
 
-    def loaded_cols(c):
-        for mat in range(2):
-            load_col(c, mat).wait()
-
-    each_col(0, n_col, load_cols)
+    def ended(ref, sem):
+        pltpu.make_async_copy(ref, ref, sem).wait()
+
+    each(0, n_col, load_cols)
 
     barrier = pltpu.get_barrier_semaphore()
 
@@ -634,7 +635,8 @@
     def _():
         greet({"fs": facing})
 
-    pl.semaphore_wait(barrier, n_grp - 1 + n_tp - 1 + 1 + inner.astype(jnp.int32))
+    with jax.named_scope("barrier"):
+        pl.semaphore_wait(barrier, n_grp - 1 + n_tp - 1 + 1 + inner.astype(jnp.int32))
 
     MAIN, OUT, ACROSS = 0, 1, 2
 
@@ -645,66 +647,76 @@
             return {"fs": mate}
         return {"grp": lax.rem(g + way - ACROSS + 1, n_grp)}
 
-    def d_copy(src, share, j, way):
+    def d_place(src, share, j):
         size = down_all.shape[1] // (n_grp * sub)
-        place = share * sub + j
-        block = down_all.at[src, pl.ds(pl.multiple_of(place * size, size), size)]
+        return down_all.at[src, pl.ds(pl.multiple_of((share * sub + j) * size, size), size)]
+
+    def d_copy(src, share, j, way, sem):
+        block = d_place(src, share, j)
         return pltpu.make_async_remote_copy(
             src_ref=block,
             dst_ref=block,
-            send_sem=d_send.at[way, src, place],
-            recv_sem=d_recv.at[src, place],
+            send_sem=d_send.at[way],
+            recv_sem=sem,
             device_id=device_of(way),
             device_id_type=MESH,
         )
 
-    def c_copy(c, src, share, way):
+    def c_copy(c, src, share, way, sem):
         size = depth // n_grp
         block = cols_all.at[c, src, pl.ds(pl.multiple_of(share * size, size), size)]
         return pltpu.make_async_remote_copy(
             src_ref=block,
             dst_ref=block,
-            send_sem=c_send.at[way, src, c, share],
-            recv_sem=c_recv.at[src, c, share],
+            send_sem=c_send.at[way],
+            recv_sem=sem,
             device_id=device_of(way),
             device_id_type=MESH,
         )
 
+    d_half = down_all.shape[1] // n_grp
+    c_half = depth // n_grp
+
     across = [ACROSS + d - 1 for d in range(1, n_grp)]
     others = [lax.rem(g + d, n_grp) for d in range(1, n_grp)]
 
-    def d_send_on(src, share, j, ways):
+    def d_send_on(src, j, ways):
         for way in ways:
-            d_copy(src, share, j, way).start()
-
-    def c_send_on(c, src, share, ways):
+            sem = d_recv.at[src, j] if way in (MAIN, OUT) else d_late.at[src]
+            d_copy(src, g, j, way, sem).start()
+
+    def d_send_late(src, share, j):
+        d_copy(src, share, j, MAIN, d_late.at[src]).start()
+
+    def c_send_on(c, src, ways):
         for way in ways:
-            c_copy(c, src, share, way).start()
+            sem = c_recv.at[src, c] if way in (MAIN, OUT) else c_late.at[c]
+            c_copy(c, src, g, way, sem).start()
+
+    def c_send_late(c, src, share):
+        c_copy(c, src, share, MAIN, c_late.at[c]).start()
 
     def d_pass(src, j, ways):
-        d_copy(src, g, j, MAIN).wait_recv()
-        d_send_on(src, g, j, ways)
+        d_copy(src, g, j, MAIN, d_recv.at[src, j]).wait_recv()
+        d_send_on(src, j, ways)
 
     def c_pass(c, src, ways):
-        c_copy(c, src, g, MAIN).wait_recv()
-        c_send_on(c, src, g, ways)
+        c_copy(c, src, g, MAIN, c_recv.at[src, c]).wait_recv()
+        c_send_on(c, src, ways)
 
     def d_rest(src):
-        for share in others:
-            for j in range(sub):
-                d_copy(src, share, j, MAIN).wait_recv()
-
-    def c_rest(c, src):
-        for share in others:
-            c_copy(c, src, share, MAIN).wait_recv()
+        ended(down_all.at[src, pl.ds(0, (n_grp - 1) * d_half)], d_late.at[src])
+
+    def c_rest(c):
+        ended(cols_all.at[c, pl.ds(0, n_fs - 1), pl.ds(0, (n_grp - 1) * c_half)], c_late.at[c])
 
     def a_copy(d):
         peer = lax.rem(t + d, n_tp)
         return pltpu.make_async_remote_copy(
             src_ref=hid_block(peer),
             dst_ref=spread.at[own_rows(t)],
-            send_sem=a_send.at[d],
-            recv_sem=a_recv.at[d],
+            send_sem=a_sem.at[0],
+            recv_sem=a_sem.at[1],
             device_id={"tp": peer},
             device_id_type=MESH,
         )
@@ -714,8 +726,8 @@
         return pltpu.make_async_remote_copy(
             src_ref=part.at[src, own_rows(peer)],
             dst_ref=red.at[d, src],
-            send_sem=r_send.at[d, src],
-            recv_sem=r_recv.at[d, src],
+            send_sem=r_sem.at[0],
+            recv_sem=r_sem.at[1],
             device_id={"tp": peer},
             device_id_type=MESH,
         )
@@ -734,8 +746,8 @@
         return pltpu.make_async_remote_copy(
             src_ref=place,
             dst_ref=place,
-            send_sem=m_send.at[whose, owner, hop, q],
-            recv_sem=m_recv.at[whose, owner, q],
+            send_sem=m_send.at[whose],
+            recv_sem=m_late.at[whose] if hop == 0 else m_recv.at[whose, owner // 2, q],
             device_id={"tp": peer},
             device_id_type=MESH,
         )
@@ -747,24 +759,20 @@
     def m_relay(whose, q):
         for hop in range(1, chips):
             owner = lax.rem(t + 2 * hop, n_tp)
-            m_copy(owner, whose, 0, q).wait_recv()
+            m_copy(owner, whose, hop, q).wait_recv()
             m_copy(owner, whose, 0, q).start()
 
-    def m_rest(whose, q):
-        for hop in range(chips):
-            m_copy(lax.rem(sibling + 2 * hop, n_tp), whose, 0, q).wait_recv()
-
-    def m_drain(whose, q):
-        for hop in range(chips):
-            m_copy(t, whose, hop, q).wait_send()
-        for hop in range(1, chips):
-            m_copy(lax.rem(t + 2 * hop, n_tp), whose, 0, q).wait_send()
+    def m_rest(whose):
+        ended(mixed_all.at[whose, pl.ds(0, chips * rows)], m_late.at[whose])
+
+    def m_drain(whose):
+        ended(mixed_all.at[whose, pl.ds(0, (2 * chips - 1) * rows)], m_send.at[whose])
 
     def g_copy(q):
         return pltpu.make_async_remote_copy(
             src_ref=mixed_all.at[0, piece_rows(t, q)],
             dst_ref=mixed_all.at[1, piece_rows(t, q)],
-            send_sem=g_send.at[q],
+            send_sem=g_send.at[0],
             recv_sem=g_recv.at[q],
             device_id={"fs": mate},
             device_id_type=MESH,
@@ -776,12 +784,19 @@
     def b_copy(c):
         return pltpu.make_async_remote_copy(
             src_ref=back.at[c - own],
-            dst_ref=out_ref.at[:, col_lanes(c)],
-            send_sem=b_send.at[c - own],
+            dst_ref=result.at[:, col_lanes(c)],
+            send_sem=b_send.at[0],
             recv_sem=b_recv.at[c - own],
             device_id={"fs": mate},
             device_id_type=MESH,
         )
+
+    def w_copy(c):
+        return pltpu.make_async_copy(
+            result.at[:, col_lanes(c)], out_ref.at[:, col_lanes(c)], w_sem.at[0]
+        )
+
+    write_mixed = pltpu.make_async_copy(mixed_all.at[0, own_rows(t)], mixed_ref, w_sem.at[1])
 
     def first_product(src):
         part[src] = jnp.dot(
@@ -792,13 +807,10 @@
 
     def take_hidden():
         load_hid.wait()
-        for d in range(1, n_tp):
-            a_copy(d).wait_recv()
+        ended(spread.at[pl.ds(0, (n_tp - 1) * rows)], a_sem.at[1])
 
     def norms():
-        for src in range(n_fs):
-            for d in range(1, n_tp):
-                r_copy(src, d).wait_recv()
+        ended(red.at[pl.ds(1, n_tp - 1)], r_sem.at[1])
         columns = []
         for src in range(n_fs):
             total = part[src, own_rows(t)].astype(jnp.float32)
@@ -817,7 +829,6 @@
             shift_ref[1:2],
         ).astype(jnp.bfloat16)
         mixed_all[0, own_rows(t)] = mixed
-        mixed_ref[...] = mixed
 
     def second_product(whose, c):
         weight = cols_all[c].reshape(n_fs * depth, 2 * lanes)
@@ -829,231 +840,260 @@
 
     @pl.when(inner)
     def _():
-        for j in range(sub):
-            d_send_on(f, g, j, (MAIN, OUT))
+        each(0, sub, lambda j: d_send_on(f, j, (MAIN, OUT)))
 
     @pl.when(outer)
     def _():
-        for share in [g] + others:
-            for j in range(sub):
-                d_send_on(f, share, j, (MAIN,))
+        each(0, sub, lambda j: d_send_on(f, j, (MAIN,)))
+        for share in others:
+            each(0, sub, lambda j: d_send_late(f, share, j))
 
     for d in range(1, n_tp):
         a_copy(d).start()
-    each_col(0, n_col, loaded_cols)
+    with jax.named_scope("loaded"):
+        ended(cols_all.at[:, f], load_sem.at[2])
 
     @pl.when(outer)
     def _():
-        each_col(0, n_col, lambda c: c_send_on(c, f, g, (MAIN,)))
-
-    ahead = min(4, n_col)
-    early = min(2, n_col)
+        each(0, n_col, lambda c: c_send_on(c, f, (MAIN,)))
+
+    with jax.named_scope("first_pass"):
+
+        @pl.when(inner)
+        def _():
+            def both(j):
+                d_pass(mate, j, (MAIN,))
+                d_pass(facing, j, [OUT] + across)
+
+            each(0, sub, both)
+            each(0, own, lambda c: c_send_on(c, f, (MAIN,)))
+
+        @pl.when(outer)
+        def _():
+            each(0, sub, lambda j: d_pass(mate, j, across))
+
+    with jax.named_scope("hidden"):
+        take_hidden()
+
+    def step(k, carry):
+        with jax.named_scope("step_wait"):
+
+            @pl.when((k == 1) & inner)
+            def _():
+                d_rest(facing)
+
+            @pl.when((k == 1) & outer)
+            def _():
+                d_rest(mate)
+
+            @pl.when((k == 2) & inner)
+            def _():
+                each(0, sub, lambda j: d_pass(beyond, j, [OUT] + across))
+                each(0, own, lambda c: c_send_on(c, f, (OUT,)))
+                d_rest(mate)
+
+            @pl.when((k == 2) & outer)
+            def _():
+                each(0, sub, lambda j: d_pass(facing, j, across))
+                d_rest(facing)
+
+            @pl.when((k == 3) & inner)
+            def _():
+                c_pass(0, mate, (MAIN,))
+                d_rest(beyond)
+
+            @pl.when((k == 3) & outer)
+            def _():
+                each(0, sub, lambda j: d_pass(beyond, j, across))
+                d_rest(beyond)
+
+        second = jnp.where(inner, facing, mate)
+        third = jnp.where(inner, mate, facing)
+        with jax.named_scope("product"):
+            first_product(
+                jnp.where(k == 0, f, jnp.where(k == 1, second, jnp.where(k == 2, third, beyond)))
+            )
+        return carry
+
+    lax.fori_loop(0, n_fs, step, 0)
+    hosted = n_col - own
+    slots = 2 * hosted
 
     @pl.when(inner)
     def _():
-        for j in range(sub):
-            d_pass(mate, j, (MAIN,))
-            d_pass(facing, j, [OUT] + across)
-        for c in range(ahead):
-            c_send_on(c, f, g, (MAIN,))
-
-    @pl.when(outer)
-    def _():
-        for j in range(sub):
-            d_pass(mate, j, across)
-
-    take_hidden()
-
-    def step(k, carry):
-        @pl.when((k == 1) & inner)
-        def _():
-            for j in range(sub):
-                d_pass(beyond, j, [OUT] + across)
-            each_col(0, own, lambda c: c_send_on(c, f, g, (OUT,)))
-            d_rest(mate)
-
-        @pl.when((k == 1) & outer)
-        def _():
-            for j in range(sub):
-                d_pass(facing, j, across)
-            d_rest(mate)
-
-        @pl.when((k == 2) & outer)
-        def _():
-            for j in range(sub):
-                d_pass(beyond, j, across)
-
-        @pl.when(k == 2)
-        def _():
-            d_rest(facing)
-
-        @pl.when((k >= 2) & (k - 2 < early) & inner)
-        def _():
-            c_pass(k - 2, mate, (MAIN,))
-
-        @pl.when(k == 3)
-        def _():
-            d_rest(beyond)
-
-        first_product(
-            jnp.where(k == 0, f, jnp.where(k == 1, mate, jnp.where(k == 2, facing, beyond)))
-        )
-        return carry
-
-    lax.fori_loop(0, n_fs, step, 0)
-    norms()
-
-    def swapped(c):
-        return c >= n_col - moved
-
-    def serve(c):
-        c_rest(c, mate)
-        c_rest(c, facing)
-        c_rest(c, beyond)
-        out_ref[:, col_lanes(c)] = second_product(0, c)
+        def begin(c):
+            @pl.when(c + 1 < own)
+            def _():
+                c_pass(c + 1, mate, (MAIN,))
+
+            c_pass(c, facing, [OUT] + across)
+
+        with jax.named_scope("begin"):
+            each(0, own, begin)
+
+    with jax.named_scope("norms"):
+        norms()
+
+    def serve(i):
+        c = jnp.where(
+            i < hosted - 1,
+            own + i,
+            jnp.where(i < hosted + 1, i - hosted + 1, jnp.where(i == hosted + 1, n_col - 1, i - hosted)),
+        )
+        with jax.named_scope("rest"):
+            c_rest(c)
 
         @pl.when(c >= own)
         def _():
-            back[c - own] = second_product(1, c)
+            with jax.named_scope("prod1"):
+                back[c - own] = second_product(1, c)
             b_copy(c).start()
 
-    def relay(c):
-        @pl.when(c >= early)
+        with jax.named_scope("prod0"):
+            result[:, col_lanes(c)] = second_product(0, c)
+        w_copy(c).start()
+
+    def feed(c):
+        @pl.when(c < n_col)
         def _():
+            c_send_on(c, f, (MAIN,))
             c_pass(c, mate, (MAIN,))
 
-        @pl.when(swapped(c))
+    def slot(s):
+        c = own + s // 2
+        src = jnp.where(s % 2 == 0, facing, beyond)
+
+        @pl.when(s % 2 == 0)
         def _():
-            c_send_on(c, mate, g, across)
-
-        @pl.when(c + ahead < n_col)
+            feed(c + 2)
+
+        with jax.named_scope("slot"):
+            c_pass(c, src, across)
+
+        when = s - (slots - 14)
+
+        @pl.when(when == 1)
         def _():
-            c_send_on(c + ahead, f, g, (MAIN,))
-
-        for src in (facing, beyond):
-            c_pass(c, src, across)
-
-            @pl.when(c < own)
-            def _():
-                c_send_on(c, src, g, (OUT,))
-
-    def relay_and_serve(c):
-        relay(c)
-        first = c - (n_col - 4)
-
-        def from_mate(q):
-            g_copy(q).wait_recv()
-            m_out(1, q)
-
-        @pl.when(c == n_col - 8)
+            with jax.named_scope("m0"):
+                for q in range(pieces):
+                    m_relay(0, q)
+
+        for q in range(pieces):
+
+            @pl.when(when == 3 + q)
+            def _():
+                with jax.named_scope("from_mate"):
+                    g_copy(q).wait_recv()
+                    m_out(1, q)
+
+            @pl.when(when == min(6 + q // 2 + q // 3, 8))
+            def _():
+                with jax.named_scope("m1"):
+                    m_relay(1, q)
+
+        @pl.when(when == 8)
         def _():
-            for q in range(pieces):
-                m_relay(0, q)
-
-        @pl.when(c == n_col - 5)
-        def _():
-            for q in range(pieces // 2):
-                from_mate(q)
-            for q in range(pieces):
-                m_rest(0, q)
-
-        @pl.when(c == n_col - 4)
-        def _():
-            for q in range(pieces // 2, pieces):
-                from_mate(q)
-            for q in range(pieces // 2):
-                m_relay(1, q)
-
-        @pl.when(c == n_col - 3)
-        def _():
-            for q in range(pieces // 2, pieces):
-                m_relay(1, q)
-            for q in range(pieces):
-                m_rest(1, q)
-
-        low = jnp.where(first < 1, 0, 2 * (first - 1))
-        high = jnp.where(first < 1, 0, jnp.where(c == n_col - 1, n_col, 2 * first))
-        each_col(low, high, serve)
+            with jax.named_scope("m_rest"):
+                m_rest(0)
+                m_rest(1)
+
+        done = jnp.maximum(when - 8, 0)
+        more = jnp.where(when == 13, n_col, jnp.maximum(when - 7, 0))
+        each(done, more, serve)
 
     @pl.when(inner)
     def _():
         for q in range(pieces):
             m_out(0, q)
-        each_col(0, n_col, relay_and_serve)
+        write_mixed.start()
+        feed(own)
+        feed(own + 1)
+        with jax.named_scope("beyond_own"):
+            each(0, own, lambda c: c_pass(c, beyond, [OUT] + across))
+        each(0, slots, slot)
 
     @pl.when(outer)
     def _():
         for q in range(pieces):
             g_copy(q).start()
             m_out(0, q)
+        write_mixed.start()
         for share in others:
-            each_col(0, n_col - moved, lambda c: c_send_on(c, f, share, (MAIN,)))
+            each(own, n_col, lambda c: c_send_late(c, f, share))
+            each(0, own, lambda c: c_send_late(c, f, share))
 
         def pass_own(c):
-            for src in (mate, facing, beyond):
-                c_pass(c, src, across)
-
-        each_col(0, own, pass_own)
-        for q in range(pieces):
-            m_relay(0, q)
-        for q in range(pieces):
-            m_rest(0, q)
+            with jax.named_scope("pass_own"):
+                c_pass(c, mate, across)
+
+        def pass_far(src):
+            def act(c):
+                with jax.named_scope("pass_far"):
+                    c_pass(c, src, across)
+
+            return act
+
+        each(0, own, pass_own)
+        each(0, own, pass_far(facing))
+        with jax.named_scope("m0"):
+            for q in range(pieces):
+                m_relay(0, q)
+            m_rest(0)
+        each(0, own, pass_far(beyond))
 
         def make_own(c):
-            for src in (mate, facing, beyond):
-                c_rest(c, src)
-            out_ref[:, col_lanes(c)] = second_product(0, c)
-
-        each_col(0, own, make_own)
-        each_col(own, n_col, lambda c: b_copy(c).wait_recv())
-
-    for d in range(1, n_tp):
-        a_copy(d).wait_send()
-        for src in range(n_fs):
-            r_copy(src, d).wait_send()
-    for q in range(pieces):
-        m_drain(0, q)
-
-    def d_sent(src, share, ways):
-        for j in range(sub):
-            for way in ways:
-                d_copy(src, share, j, way).wait_send()
-
-    def c_sent(low, high, src, share, ways):
-        def act(c):
-            for way in ways:
-                c_copy(c, src, share, way).wait_send()
-
-        each_col(low, high, act)
-
-    @pl.when(inner)
-    def _():
-        d_sent(f, g, (MAIN, OUT))
-        d_sent(mate, g, (MAIN,))
-        c_sent(0, n_col, f, g, (MAIN,))
-        c_sent(0, n_col, mate, g, (MAIN,))
-        c_sent(0, own, f, g, (OUT,))
-        c_sent(n_col - moved, n_col, mate, g, across)
-        for src in (facing, beyond):
-            d_sent(src, g, [OUT] + across)
-            c_sent(0, n_col, src, g, across)
-            c_sent(0, own, src, g, (OUT,))
-        for q in range(pieces):
-            m_drain(1, q)
-        each_col(own, n_col, lambda c: b_copy(c).wait_send())
-
-    @pl.when(outer)
-    def _():
-        for share in [g] + others:
-            d_sent(f, share, (MAIN,))
-        c_sent(0, n_col, f, g, (MAIN,))
-        for share in others:
-            c_sent(0, n_col - moved, f, share, (MAIN,))
-        for src in (mate, facing, beyond):
-            d_sent(src, g, across)
-            c_sent(0, own, src, g, across)
-        for q in range(pieces):
-            g_copy(q).wait_send()
+            with jax.named_scope("rest"):
+                c_rest(c)
+            with jax.named_scope("prod0"):
+                result[:, col_lanes(c)] = second_product(0, c)
+            w_copy(c).start()
+
+        each(0, own, make_own)
+        with jax.named_scope("b_wait"):
+
+            def take_back(c):
+                b_copy(c).wait_recv()
+                w_copy(c).start()
+
+            each(own, n_col, take_back)
+
+    def d_sent(blocks, ways):
+        for way in ways:
+            ended(down_all.at[pl.ds(0, blocks), pl.ds(0, d_half)], d_send.at[way])
+
+    def c_sent(columns, blocks, ways):
+        for way in ways:
+            ended(
+                cols_all.at[pl.ds(0, columns), pl.ds(0, blocks), pl.ds(0, c_half)], c_send.at[way]
+            )
+
+    with jax.named_scope("drain"):
+        ended(spread.at[pl.ds(0, (n_tp - 1) * rows)], a_sem.at[0])
+        ended(red.at[pl.ds(1, n_tp - 1)], r_sem.at[0])
+        m_drain(0)
+
+        @pl.when(inner)
+        def _():
+            d_sent(2, (MAIN,))
+            d_sent(3, (OUT,))
+            d_sent(2, across)
+            c_sent(n_col, 2, (MAIN,))
+            c_sent(own, 3, (OUT,))
+            c_sent(n_col, 2, across)
+            m_drain(1)
+            ended(back, b_send.at[0])
+
+        @pl.when(outer)
+        def _():
+            ended(down_all.at[f], d_send.at[MAIN])
+            ended(cols_all.at[:, f], c_send.at[MAIN])
+            d_sent(3, across)
+            c_sent(own, 3, across)
+            ended(mixed_all.at[0, own_rows(t)], g_send.at[0])
+
+    with jax.named_scope("written"):
+        write_mixed.wait()
+        ended(result, w_sem.at[0])
 
 
 def paired_call(sizes, arguments):
@@ -1065,21 +1105,21 @@
     tokens = rows * n_tp
     lanes = 128
     n_col = width // lanes
-    sub = 4
-    own = max(1, n_col * 4 // 11)
-    moved = 1
+    share = down_weight.shape[0] // (n_grp * 16)
+    sub = max(n for n in range(1, 12) if share % n == 0)
+    own = n_col * 4 // 11
     pieces = 4
     vmem = pl.BlockSpec(memory_space=pltpu.VMEM)
     anywhere = pl.BlockSpec(memory_space=pl.ANY)
     dma = pltpu.SemaphoreType.DMA
     return pl.pallas_call(
-        functools.partial(paired_kernel, (n_grp, n_fs, n_tp, sub, own, moved, pieces)),
+        functools.partial(paired_kernel, (n_grp, n_fs, n_tp, sub, own, pieces)),
         out_shape=(
             jax.ShapeDtypeStruct((rows, model), jnp.bfloat16),
             jax.ShapeDtypeStruct((tokens, width), jnp.bfloat16),
         ),
         in_specs=[vmem, anywhere, anywhere, vmem, vmem, vmem, anywhere, anywhere],
-        out_specs=(vmem, vmem),
+        out_specs=(anywhere, anywhere),
         scratch_shapes=[
             pltpu.VMEM((n_fs,) + down_weight.shape, jnp.bfloat16),
             pltpu.VMEM((n_col, n_fs, depth, 2 * lanes), jnp.bfloat16),
@@ -1088,22 +1128,24 @@
             pltpu.VMEM((n_tp, n_fs, rows, cols), jnp.bfloat16),
             pltpu.VMEM((2, tokens, model), jnp.bfloat16),
             pltpu.VMEM((n_col - own, tokens, lanes), jnp.bfloat16),
+            pltpu.VMEM((tokens, width), jnp.bfloat16),
+            dma((3,)),
+            dma((1 + n_grp,)),
+            dma((n_fs, sub)),
+            dma((n_fs,)),
+            dma((1 + n_grp,)),
+            dma((n_fs, n_col)),
+            dma((n_col,)),
             dma((2,)),
-            dma((n_col, 2)),
-            dma((1 + n_grp, n_fs, n_grp * sub)),
-            dma((n_fs, n_grp * sub)),
-            dma((1 + n_grp, n_fs, n_col, n_grp)),
-            dma((n_fs, n_col, n_grp)),
-            dma((n_tp,)),
-            dma((n_tp,)),
-            dma((n_tp, n_fs)),
-            dma((n_tp, n_fs)),
-            dma((2, n_tp, n_tp // 2, pieces)),
-            dma((2, n_tp, pieces)),
+            dma((2,)),
+            dma((2,)),
+            dma((2, n_tp // 2, pieces)),
+            dma((2,)),
+            dma((1,)),
             dma((pieces,)),
-            dma((pieces,)),
+            dma((1,)),
             dma((n_col - own,)),
-            dma((n_col - own,)),
+            dma((2,)),
         ],
         compiler_params=pltpu.CompilerParams(
             collective_id=0, has_side_effects=True, vmem_limit_bytes=60 * 1024 * 1024
@@ -1119,9 +1161,9 @@
         n_fs == 4
         and n_tp % 2 == 0
         and width % 128 == 0
-        and width // 128 >= 9
+        and width // 128 >= 10
         and depth % (n_grp * 32) == 0
-        and down_weight.shape[0] % (n_grp * 4 * 16) == 0
+        and down_weight.shape[0] % (n_grp * 16) == 0
         and residual_in.shape[0] % (4 * 16) == 0
     )
 

time: 152 us -> 120 us (0.79)
  Pallas kernels: 147 us -> 115 us
    pallas_call x1, Pallas kernels: 147 us -> 115 us  [paired_call(): pl.pallas_call(functools.partial(paired_kernel, (n_grp, n_fs, n_tp, sub,...]
where the time goes in v2:
time: 120 us
  Pallas kernels  115 us (96%)
  local copies, waits for them, and re-layouts  4.45 us (4%)
    pallas_call x1, Pallas kernels, paired_call(): pl.pallas_call(functools.partial(paired_kernel, (n_grp, n_fs, n_tp, sub,...  115 us
    unnamed x2, local copies, waits for them, and re-layouts  4.45 us

profile of v2, /device:TPU:0, one launch (start us, length us, event | category | flops | bytes accessed | tf_op | source)
XLA Modules:
  0.0 119.6 jit_solution(1777571501850045921)
XLA Ops:
  0.6 114.5 %paired_half_steps.1 = (bf16[128,2048]{1,0:T(8,128)(2,1)}, bf16[512,1408]{1,0:T(8,128)(2,1)}) custom-call(bf16[128,2048]{1,0:T(8,128)(2,1)} %res_ref.1, bf16[128,5632]{1,0:T(8,128)(2,1)} %hid_ref.1, bf16[1408,512]{1,0:T(8,128)(2,1)} %down_ref.1, bf16[128,2048]{1,0:T(8,128)(2,1)} %mix_ref.1, f32[2,2048]{1,0:T(2,128)} %gain_ref.1, f32[2,2048]{1,0:T(2,128)} %shift_ref.1, ...), custom_call_target="tpu_custom_call" | custom-call | tf_op jit(solution)/shard_map/paired_half_steps/pallas_call | solution.py:1115
  115.1 1.9 %copy.12 = bf16[128,2048]{1,0:T(8,128)(2,1)} copy(bf16[128,2048]{1,0:T(8,128)(2,1)} %get-tuple-element.4) | data formatting | bytes 1048576
  117.0 2.6 %copy.13 = bf16[512,1408]{1,0:T(8,128)(2,1)} copy(bf16[512,1408]{1,0:T(8,128)(2,1)} %get-tuple-element.5) | data formatting | bytes 2883584

commit v3 on v2

--- a/solution.py
+++ b/solution.py
@@ -551,7 +551,10 @@
     red,
     mixed_all,
     back,
-    result,
+    res_now,
+    mix_now,
+    gain_now,
+    shift_now,
     load_sem,
     d_send,
     d_recv,
@@ -568,9 +571,8 @@
     g_recv,
     b_send,
     b_recv,
-    w_sem,
 ):
-    n_grp, n_fs, n_tp, sub, own, pieces = sizes
+    n_grp, n_fs, n_tp, sub, own, pieces, ahead, parts = sizes
     g, f, t = lax.axis_index("grp"), lax.axis_index("fs"), lax.axis_index("tp")
     rows = res_ref.shape[0]
     width = gate_ref.shape[1]
@@ -603,6 +605,19 @@
 
     load_down.start()
     load_hid.start()
+    row_loads = [
+        pltpu.make_async_copy(whole, now, load_sem.at[3 + k])
+        for k, (whole, now) in enumerate(
+            (
+                (res_ref, res_now),
+                (mix_ref, mix_now),
+                (gain_ref, gain_now),
+                (shift_ref, shift_now),
+            )
+        )
+    ]
+    for load in row_loads:
+        load.start()
 
     def each(low, high, act):
         def body(c, carry):
@@ -662,18 +677,37 @@
             device_id_type=MESH,
         )
 
-    def c_copy(c, src, share, way, sem):
-        size = depth // n_grp
-        block = cols_all.at[c, src, pl.ds(pl.multiple_of(share * size, size), size)]
+    def c_copy(c, src, share, part_of, way, sem, count=None):
+        whole = depth // n_grp
+        size = whole if part_of is None else whole // parts
+        start = share * whole + (0 if part_of is None else part_of * size)
+        block = cols_all.at[c, src, pl.ds(pl.multiple_of(start, size), size)]
         return pltpu.make_async_remote_copy(
             src_ref=block,
             dst_ref=block,
-            send_sem=c_send.at[way],
+            send_sem=c_send.at[way if count is None else count],
             recv_sem=sem,
             device_id=device_of(way),
             device_id_type=MESH,
         )
 
+    def place_at(receiver, src):
+        return src - (src > receiver).astype(jnp.int32)
+
+    def receiver_of(way):
+        return jnp.where(inner, facing, mate) if way == MAIN else mate
+
+    def moved_copy(d):
+        block = cols_all.at[own - 1, mate, pl.ds(pl.multiple_of(g * c_half, c_half), c_half)]
+        return pltpu.make_async_remote_copy(
+            src_ref=block,
+            dst_ref=block,
+            send_sem=c_send.at[ACROSS + n_grp - 2 + d],
+            recv_sem=c_late.at[own - 1],
+            device_id={"grp": lax.rem(g + d, n_grp)},
+            device_id_type=MESH,
+        )
+
     d_half = down_all.shape[1] // n_grp
     c_half = depth // n_grp
 
@@ -682,27 +716,39 @@
 
     def d_send_on(src, j, ways):
         for way in ways:
-            sem = d_recv.at[src, j] if way in (MAIN, OUT) else d_late.at[src]
+            if way in (MAIN, OUT):
+                sem = d_recv.at[place_at(receiver_of(way), src), j]
+            else:
+                sem = d_late.at[src]
             d_copy(src, g, j, way, sem).start()
 
     def d_send_late(src, share, j):
         d_copy(src, share, j, MAIN, d_late.at[src]).start()
 
+    def c_part_on(c, src, k, ways):
+        for way in ways:
+            if way in (MAIN, OUT):
+                sem = c_recv.at[place_at(receiver_of(way), src), c * parts + k]
+            else:
+                sem = c_late.at[c]
+            c_copy(c, src, g, k, way, sem).start()
+
     def c_send_on(c, src, ways):
-        for way in ways:
-            sem = c_recv.at[src, c] if way in (MAIN, OUT) else c_late.at[c]
-            c_copy(c, src, g, way, sem).start()
+        for k in range(parts):
+            c_part_on(c, src, k, ways)
 
     def c_send_late(c, src, share):
-        c_copy(c, src, share, MAIN, c_late.at[c]).start()
+        c_copy(c, src, share, None, MAIN, c_late.at[c], ACROSS + n_grp - 1).start()
 
     def d_pass(src, j, ways):
-        d_copy(src, g, j, MAIN, d_recv.at[src, j]).wait_recv()
+        d_copy(src, g, j, MAIN, d_recv.at[place_at(f, src), j]).wait_recv()
         d_send_on(src, j, ways)
 
     def c_pass(c, src, ways):
-        c_copy(c, src, g, MAIN, c_recv.at[src, c]).wait_recv()
-        c_send_on(c, src, ways)
+        for k in range(parts):
+            sem = c_recv.at[place_at(f, src), c * parts + k]
+            c_copy(c, src, g, k, MAIN, sem).wait_recv()
+            c_part_on(c, src, k, ways)
 
     def d_rest(src):
         ended(down_all.at[src, pl.ds(0, (n_grp - 1) * d_half)], d_late.at[src])
@@ -747,7 +793,7 @@
             src_ref=place,
             dst_ref=place,
             send_sem=m_send.at[whose],
-            recv_sem=m_late.at[whose] if hop == 0 else m_recv.at[whose, owner // 2, q],
+            recv_sem=m_late.at[whose] if hop == 0 else m_recv.at[owner // 2, whose * (q + 1)],
             device_id={"tp": peer},
             device_id_type=MESH,
         )
@@ -761,6 +807,13 @@
             owner = lax.rem(t + 2 * hop, n_tp)
             m_copy(owner, whose, hop, q).wait_recv()
             m_copy(owner, whose, 0, q).start()
+
+    def m_relay_all():
+        for hop in range(1, chips):
+            owner = lax.rem(t + 2 * hop, n_tp)
+            ended(mixed_all.at[0, own_rows(owner)], m_recv.at[owner // 2, 0])
+            for q in range(pieces):
+                m_copy(owner, 0, 0, q).start()
 
     def m_rest(whose):
         ended(mixed_all.at[whose, pl.ds(0, chips * rows)], m_late.at[whose])
@@ -781,22 +834,20 @@
     def col_lanes(c):
         return pl.ds(pl.multiple_of(c * lanes, lanes), lanes)
 
-    def b_copy(c):
+    tile = n_tp * rows // 2
+
+    def tile_rows(h):
+        return pl.ds(pl.multiple_of(h * tile, tile), tile)
+
+    def b_copy(c, span=slice(None)):
         return pltpu.make_async_remote_copy(
-            src_ref=back.at[c - own],
-            dst_ref=result.at[:, col_lanes(c)],
+            src_ref=back.at[c - own, span],
+            dst_ref=out_ref.at[span, col_lanes(c)],
             send_sem=b_send.at[0],
-            recv_sem=b_recv.at[c - own],
+            recv_sem=b_recv.at[0],
             device_id={"fs": mate},
             device_id_type=MESH,
         )
-
-    def w_copy(c):
-        return pltpu.make_async_copy(
-            result.at[:, col_lanes(c)], out_ref.at[:, col_lanes(c)], w_sem.at[0]
-        )
-
-    write_mixed = pltpu.make_async_copy(mixed_all.at[0, own_rows(t)], mixed_ref, w_sem.at[1])
 
     def first_product(src):
         part[src] = jnp.dot(
@@ -809,30 +860,36 @@
         load_hid.wait()
         ended(spread.at[pl.ds(0, (n_tp - 1) * rows)], a_sem.at[1])
 
-    def norms():
+    def sums_in():
         ended(red.at[pl.ds(1, n_tp - 1)], r_sem.at[1])
+        for load in row_loads:
+            load.wait()
+
+    def norms(q):
+        here = pl.ds(pl.multiple_of(q * piece, piece), piece)
         columns = []
         for src in range(n_fs):
-            total = part[src, own_rows(t)].astype(jnp.float32)
+            total = part[src, piece_rows(t, q)].astype(jnp.float32)
             for d in range(1, n_tp):
-                total = total + red[d, src].astype(jnp.float32)
+                total = total + red[d, src, here].astype(jnp.float32)
             columns.append(total)
         branch = jnp.concatenate(columns, axis=1)
         first = layer_norm(
-            jnp.sqrt(2.0) * res_ref[...].astype(jnp.float32) + 0.5 * branch,
-            gain_ref[0:1],
-            shift_ref[0:1],
+            jnp.sqrt(2.0) * res_now[here].astype(jnp.float32) + 0.5 * branch,
+            gain_now[0:1],
+            shift_now[0:1],
         )
         mixed = layer_norm(
-            jnp.sqrt(2.0) * first + mix_ref[...].astype(jnp.float32),
-            gain_ref[1:2],
-            shift_ref[1:2],
+            jnp.sqrt(2.0) * first + mix_now[here].astype(jnp.float32),
+            gain_now[1:2],
+            shift_now[1:2],
         ).astype(jnp.bfloat16)
-        mixed_all[0, own_rows(t)] = mixed
-
-    def second_product(whose, c):
+        mixed_all[0, piece_rows(t, q)] = mixed
+        mixed_ref[here] = mixed
+
+    def second_product(whose, c, span=slice(None)):
         weight = cols_all[c].reshape(n_fs * depth, 2 * lanes)
-        total = jnp.dot(mixed_all[whose], weight, preferred_element_type=jnp.float32)
+        total = jnp.dot(mixed_all[whose, span], weight, preferred_element_type=jnp.float32)
         gate = total[:, :lanes]
         return (gate / (1.0 + jnp.exp(-gate)) * total[:, lanes:]).astype(jnp.bfloat16)
 
@@ -855,7 +912,7 @@
 
     @pl.when(outer)
     def _():
-        each(0, n_col, lambda c: c_send_on(c, f, (MAIN,)))
+        each(0, ahead, lambda c: c_send_on(c, f, (MAIN,)))
 
     with jax.named_scope("first_pass"):
 
@@ -875,36 +932,43 @@
     with jax.named_scope("hidden"):
         take_hidden()
 
+    part_way = min(4, sub)
+
     def step(k, carry):
         with jax.named_scope("step_wait"):
 
             @pl.when((k == 1) & inner)
             def _():
+                each(0, part_way, lambda j: d_pass(beyond, j, [OUT] + across))
                 d_rest(facing)
 
             @pl.when((k == 1) & outer)
             def _():
+                each(0, part_way, lambda j: d_pass(facing, j, across))
                 d_rest(mate)
 
             @pl.when((k == 2) & inner)
             def _():
-                each(0, sub, lambda j: d_pass(beyond, j, [OUT] + across))
+                each(part_way, sub, lambda j: d_pass(beyond, j, [OUT] + across))
                 each(0, own, lambda c: c_send_on(c, f, (OUT,)))
                 d_rest(mate)
 
             @pl.when((k == 2) & outer)
             def _():
-                each(0, sub, lambda j: d_pass(facing, j, across))
+                each(part_way, sub, lambda j: d_pass(facing, j, across))
+                each(0, part_way, lambda j: d_pass(beyond, j, across))
                 d_rest(facing)
 
             @pl.when((k == 3) & inner)
             def _():
+                c_pass(0, facing, [OUT] + across)
                 c_pass(0, mate, (MAIN,))
+                c_pass(1, facing, [OUT] + across)
                 d_rest(beyond)
 
             @pl.when((k == 3) & outer)
             def _():
-                each(0, sub, lambda j: d_pass(beyond, j, across))
+                each(part_way, sub, lambda j: d_pass(beyond, j, across))
                 d_rest(beyond)
 
         second = jnp.where(inner, facing, mate)
@@ -922,42 +986,69 @@
     @pl.when(inner)
     def _():
         def begin(c):
-            @pl.when(c + 1 < own)
-            def _():
-                c_pass(c + 1, mate, (MAIN,))
-
-            c_pass(c, facing, [OUT] + across)
+            @pl.when(c > 0)
+            def _():
+                c_pass(c, mate, (MAIN,))
+
+            @pl.when(c > 1)
+            def _():
+                c_pass(c, facing, [OUT] + across)
 
         with jax.named_scope("begin"):
             each(0, own, begin)
 
-    with jax.named_scope("norms"):
-        norms()
+    with jax.named_scope("sums_in"):
+        sums_in()
+
+    def norms_out(q):
+        with jax.named_scope("norms"):
+            norms(q)
+
+        @pl.when(outer)
+        def _():
+            g_copy(q).start()
+
+        m_out(0, q)
+
+        @pl.when(inner & (q == pieces // 2 - 1))
+        def _():
+            c_pass(0, beyond, [OUT] + across)
+            feed(own)
+
+    def feed(c):
+        @pl.when(c < n_col)
+        def _():
+            c_send_on(c, f, (MAIN,))
+            c_pass(c, mate, (MAIN,))
+
+    each(0, pieces, norms_out)
 
     def serve(i):
         c = jnp.where(
             i < hosted - 1,
             own + i,
-            jnp.where(i < hosted + 1, i - hosted + 1, jnp.where(i == hosted + 1, n_col - 1, i - hosted)),
+            jnp.where(i == hosted - 1, 0, jnp.where(i == hosted, n_col - 1, i - hosted)),
         )
         with jax.named_scope("rest"):
             c_rest(c)
 
-        @pl.when(c >= own)
+        @pl.when((c >= own) & (c < n_col - 1))
         def _():
             with jax.named_scope("prod1"):
                 back[c - own] = second_product(1, c)
             b_copy(c).start()
 
+        @pl.when(c == n_col - 1)
+        def _():
+            def half(h):
+                span = tile_rows(h)
+                back[c - own, span] = second_product(1, c, span)
+                b_copy(c, span).start()
+
+            each(0, 2, half)
+
         with jax.named_scope("prod0"):
-            result[:, col_lanes(c)] = second_product(0, c)
-        w_copy(c).start()
-
-    def feed(c):
-        @pl.when(c < n_col)
-        def _():
-            c_send_on(c, f, (MAIN,))
-            c_pass(c, mate, (MAIN,))
+            out_ref[:, col_lanes(c)] = second_product(0, c)
 
     def slot(s):
         c = own + s // 2
@@ -975,52 +1066,50 @@
         @pl.when(when == 1)
         def _():
             with jax.named_scope("m0"):
-                for q in range(pieces):
-                    m_relay(0, q)
+                m_relay_all()
 
         for q in range(pieces):
 
-            @pl.when(when == 3 + q)
+            @pl.when(when == 2 + q)
             def _():
                 with jax.named_scope("from_mate"):
                     g_copy(q).wait_recv()
                     m_out(1, q)
 
-            @pl.when(when == min(6 + q // 2 + q // 3, 8))
+            @pl.when(when == min(5 + q // 2 + q // 3, 7))
             def _():
                 with jax.named_scope("m1"):
                     m_relay(1, q)
 
-        @pl.when(when == 8)
+        @pl.when(when == 7)
         def _():
             with jax.named_scope("m_rest"):
                 m_rest(0)
                 m_rest(1)
 
-        done = jnp.maximum(when - 8, 0)
-        more = jnp.where(when == 13, n_col, jnp.maximum(when - 7, 0))
+        @pl.when(s == slots - 1)
+        def _():
+            for d in range(1, n_grp):
+                moved_copy(d).start()
+
+        done = jnp.clip(when - 7, 0, hosted - 2)
+        more = jnp.where(when == 13, n_col, jnp.clip(when - 6, 0, hosted - 2))
         each(done, more, serve)
 
     @pl.when(inner)
     def _():
-        for q in range(pieces):
-            m_out(0, q)
-        write_mixed.start()
-        feed(own)
-        feed(own + 1)
         with jax.named_scope("beyond_own"):
-            each(0, own, lambda c: c_pass(c, beyond, [OUT] + across))
+            c_pass(1, beyond, [OUT] + across)
+            feed(own + 1)
+            each(2, own, lambda c: c_pass(c, beyond, [OUT] + across))
         each(0, slots, slot)
 
     @pl.when(outer)
     def _():
-        for q in range(pieces):
-            g_copy(q).start()
-            m_out(0, q)
-        write_mixed.start()
+        each(ahead, n_col, lambda c: c_send_on(c, f, (MAIN,)))
         for share in others:
             each(own, n_col, lambda c: c_send_late(c, f, share))
-            each(0, own, lambda c: c_send_late(c, f, share))
+            each(0, own - 1, lambda c: c_send_late(c, f, share))
 
         def pass_own(c):
             with jax.named_scope("pass_own"):
@@ -1036,8 +1125,7 @@
         each(0, own, pass_own)
         each(0, own, pass_far(facing))
         with jax.named_scope("m0"):
-            for q in range(pieces):
-                m_relay(0, q)
+            m_relay_all()
             m_rest(0)
         each(0, own, pass_far(beyond))
 
@@ -1045,17 +1133,11 @@
             with jax.named_scope("rest"):
                 c_rest(c)
             with jax.named_scope("prod0"):
-                result[:, col_lanes(c)] = second_product(0, c)
-            w_copy(c).start()
+                out_ref[:, col_lanes(c)] = second_product(0, c)
 
         each(0, own, make_own)
         with jax.named_scope("b_wait"):
-
-            def take_back(c):
-                b_copy(c).wait_recv()
-                w_copy(c).start()
-
-            each(own, n_col, take_back)
+            ended(back, b_recv.at[0])
 
     def d_sent(blocks, ways):
         for way in ways:
@@ -1080,20 +1162,23 @@
             c_sent(n_col, 2, (MAIN,))
             c_sent(own, 3, (OUT,))
             c_sent(n_col, 2, across)
+            for d in range(1, n_grp):
+                moved_copy(d).wait_send()
             m_drain(1)
             ended(back, b_send.at[0])
 
         @pl.when(outer)
         def _():
             ended(down_all.at[f], d_send.at[MAIN])
-            ended(cols_all.at[:, f], c_send.at[MAIN])
+            c_sent(n_col, 1, (MAIN,))
+            late = n_col - 1
+            ended(
+                cols_all.at[pl.ds(0, late), 0, pl.ds(0, (n_grp - 1) * c_half)],
+                c_send.at[ACROSS + n_grp - 1],
+            )
             d_sent(3, across)
             c_sent(own, 3, across)
             ended(mixed_all.at[0, own_rows(t)], g_send.at[0])
-
-    with jax.named_scope("written"):
-        write_mixed.wait()
-        ended(result, w_sem.at[0])
 
 
 def paired_call(sizes, arguments):
@@ -1109,17 +1194,19 @@
     sub = max(n for n in range(1, 12) if share % n == 0)
     own = n_col * 4 // 11
     pieces = 4
+    ahead = n_col - 1
+    parts = 2
     vmem = pl.BlockSpec(memory_space=pltpu.VMEM)
-    anywhere = pl.BlockSpec(memory_space=pl.ANY)
+    hbm = pl.BlockSpec(memory_space=pltpu.HBM)
     dma = pltpu.SemaphoreType.DMA
     return pl.pallas_call(
-        functools.partial(paired_kernel, (n_grp, n_fs, n_tp, sub, own, pieces)),
+        functools.partial(paired_kernel, (n_grp, n_fs, n_tp, sub, own, pieces, ahead, parts)),
         out_shape=(
             jax.ShapeDtypeStruct((rows, model), jnp.bfloat16),
             jax.ShapeDtypeStruct((tokens, width), jnp.bfloat16),
         ),
-        in_specs=[vmem, anywhere, anywhere, vmem, vmem, vmem, anywhere, anywhere],
-        out_specs=(anywhere, anywhere),
+        in_specs=[hbm] * 8,
+        out_specs=(vmem, vmem),
         scratch_shapes=[
             pltpu.VMEM((n_fs,) + down_weight.shape, jnp.bfloat16),
             pltpu.VMEM((n_col, n_fs, depth, 2 * lanes), jnp.bfloat16),
@@ -1128,30 +1215,32 @@
             pltpu.VMEM((n_tp, n_fs, rows, cols), jnp.bfloat16),
             pltpu.VMEM((2, tokens, model), jnp.bfloat16),
             pltpu.VMEM((n_col - own, tokens, lanes), jnp.bfloat16),
-            pltpu.VMEM((tokens, width), jnp.bfloat16),
-            dma((3,)),
+            pltpu.VMEM((rows, model), jnp.bfloat16),
+            pltpu.VMEM((rows, model), jnp.bfloat16),
+            pltpu.VMEM((2, model), jnp.float32),
+            pltpu.VMEM((2, model), jnp.float32),
+            dma((7,)),
             dma((1 + n_grp,)),
-            dma((n_fs, sub)),
+            dma((n_fs - 1, sub)),
             dma((n_fs,)),
-            dma((1 + n_grp,)),
-            dma((n_fs, n_col)),
+            dma((2 * n_grp,)),
+            dma((n_fs - 1, n_col * parts)),
             dma((n_col,)),
             dma((2,)),
             dma((2,)),
             dma((2,)),
-            dma((2, n_tp // 2, pieces)),
+            dma((n_tp // 2, 1 + pieces)),
             dma((2,)),
             dma((1,)),
             dma((pieces,)),
             dma((1,)),
-            dma((n_col - own,)),
-            dma((2,)),
+            dma((1,)),
         ],
         compiler_params=pltpu.CompilerParams(
-            collective_id=0, has_side_effects=True, vmem_limit_bytes=60 * 1024 * 1024
+            collective_id=0, has_side_effects=True, vmem_limit_bytes=48 * 1024 * 1024
         ),
         name="paired_half_steps",
-    )(*arguments)
+    )(*(pltpu.with_memory_space_constraint(a, pltpu.HBM) for a in arguments))
 
 
 def fits_pairs(sizes, residual_in, down_weight, gate_weight):
@@ -1162,7 +1251,7 @@
         and n_tp % 2 == 0
         and width % 128 == 0
         and width // 128 >= 10
-        and depth % (n_grp * 32) == 0
+        and depth % (n_grp * 2 * 16) == 0
         and down_weight.shape[0] % (n_grp * 16) == 0
         and residual_in.shape[0] % (4 * 16) == 0
     )

time: 120 us -> 114 us (0.950)
  Pallas kernels: 115 us -> 111 us
  local copies, waits for them, and re-layouts: 4.45 us -> 1.89 us
    pallas_call x1, Pallas kernels: 115 us -> 111 us  [paired_call(): pl.pallas_call(functools.partial(paired_kernel, (n_grp, n_fs, n_tp, sub,...]
    unnamed x2, local copies, waits for them, and re-layouts: 4.45 us -> 1.89 us
where the time goes in v3:
time: 114 us; the launch traced here: 113 us
  Pallas kernels  111 us (97%)
  local copies, waits for them, and re-layouts  1.89 us (2%)
    pallas_call x1, Pallas kernels, paired_call(): pl.pallas_call(functools.partial(paired_kernel, (n_grp, n_fs, n_tp, sub,...  111 us

profile of v3, /device:TPU:0, one launch (start us, length us, event | category | flops | bytes accessed | tf_op | source)
XLA Modules:
  0.0 113.4 jit_solution(9387268617171860975)
XLA Ops:
  0.6 110.9 %paired_half_steps.1 = (bf16[128,2048]{1,0:T(8,128)(2,1)S(1)}, bf16[512,1408]{1,0:T(8,128)(2,1)S(1)}) custom-call(bf16[128,2048]{1,0:T(8,128)(2,1)} %res_ref.1, bf16[128,5632]{1,0:T(8,128)(2,1)} %hid_ref.1, bf16[1408,512]{1,0:T(8,128)(2,1)} %down_ref.1, bf16[128,2048]{1,0:T(8,128)(2,1)} %mix_ref.1, f32[2,2048]{1,0:T(2,128)} %gain_ref.1, ...), custom_call_target="tpu_custom_call" | custom-call | tf_op jit(solution)/shard_map/paired_half_steps/pallas_call | solution.py:1202
  111.5 0.8 copy.12
  112.3 1.1 copy.13

commit v4 on v3

--- a/solution.py
+++ b/solution.py
@@ -572,7 +572,7 @@
     b_send,
     b_recv,
 ):
-    n_grp, n_fs, n_tp, sub, own, pieces, ahead, parts = sizes
+    n_grp, n_fs, n_tp, sub, own, pieces, ahead, moved = sizes
     g, f, t = lax.axis_index("grp"), lax.axis_index("fs"), lax.axis_index("tp")
     rows = res_ref.shape[0]
     width = gate_ref.shape[1]
@@ -654,6 +654,7 @@
         pl.semaphore_wait(barrier, n_grp - 1 + n_tp - 1 + 1 + inner.astype(jnp.int32))
 
     MAIN, OUT, ACROSS = 0, 1, 2
+    TAIL, LATE, LAST = n_grp, 2 * n_grp, 2 * n_grp + 1
 
     def device_of(way):
         if way == MAIN:
@@ -677,11 +678,12 @@
             device_id_type=MESH,
         )
 
-    def c_copy(c, src, share, part_of, way, sem, count=None):
+    def c_copy(c, src, share, part_of, way, sem, count=None, parts=1):
         whole = depth // n_grp
-        size = whole if part_of is None else whole // parts
-        start = share * whole + (0 if part_of is None else part_of * size)
-        block = cols_all.at[c, src, pl.ds(pl.multiple_of(start, size), size)]
+        size = whole // parts
+        block = cols_all.at[
+            c, src, pl.ds(pl.multiple_of(share * whole + part_of * size, size), size)
+        ]
         return pltpu.make_async_remote_copy(
             src_ref=block,
             dst_ref=block,
@@ -697,16 +699,17 @@
     def receiver_of(way):
         return jnp.where(inner, facing, mate) if way == MAIN else mate
 
-    def moved_copy(d):
-        block = cols_all.at[own - 1, mate, pl.ds(pl.multiple_of(g * c_half, c_half), c_half)]
-        return pltpu.make_async_remote_copy(
-            src_ref=block,
-            dst_ref=block,
-            send_sem=c_send.at[ACROSS + n_grp - 2 + d],
-            recv_sem=c_late.at[own - 1],
-            device_id={"grp": lax.rem(g + d, n_grp)},
-            device_id_type=MESH,
-        )
+    def tail(c, src):
+        for d in range(1, n_grp):
+            c_copy(c, src, g, 0, ACROSS + d - 1, c_late.at[c], TAIL + d).start()
+
+    def straight_copies():
+        last = n_col - 1
+        copies = []
+        for share in others:
+            copies.append(c_copy(last, f, share, 0, MAIN, c_late.at[last], LATE))
+            copies.append(c_copy(own - 1, f, share, 0, MAIN, c_late.at[own - 1], LAST))
+        return copies
 
     d_half = down_all.shape[1] // n_grp
     c_half = depth // n_grp
@@ -725,30 +728,34 @@
     def d_send_late(src, share, j):
         d_copy(src, share, j, MAIN, d_late.at[src]).start()
 
-    def c_part_on(c, src, k, ways):
+    def c_part_on(c, src, k, ways, parts):
         for way in ways:
             if way in (MAIN, OUT):
-                sem = c_recv.at[place_at(receiver_of(way), src), c * parts + k]
+                sem = c_recv.at[place_at(receiver_of(way), src), c + k]
             else:
                 sem = c_late.at[c]
-            c_copy(c, src, g, k, way, sem).start()
-
-    def c_send_on(c, src, ways):
+            c_copy(c, src, g, k, way, sem, parts=parts).start()
+
+    def c_send_on(c, src, ways, parts=1):
         for k in range(parts):
-            c_part_on(c, src, k, ways)
+            c_part_on(c, src, k, ways, parts)
 
     def c_send_late(c, src, share):
-        c_copy(c, src, share, None, MAIN, c_late.at[c], ACROSS + n_grp - 1).start()
+        c_copy(c, src, share, 0, MAIN, c_late.at[c], LATE).start()
 
     def d_pass(src, j, ways):
         d_copy(src, g, j, MAIN, d_recv.at[place_at(f, src), j]).wait_recv()
         d_send_on(src, j, ways)
 
-    def c_pass(c, src, ways):
+    def c_pass(c, src, ways, parts=1):
         for k in range(parts):
-            sem = c_recv.at[place_at(f, src), c * parts + k]
-            c_copy(c, src, g, k, MAIN, sem).wait_recv()
-            c_part_on(c, src, k, ways)
+            sem = c_recv.at[place_at(f, src), c + k]
+            c_copy(c, src, g, k, MAIN, sem, parts=parts).wait_recv()
+            c_part_on(c, src, k, ways, parts)
+
+    def c_pass_part(c, src, k):
+        sem = c_recv.at[place_at(f, src), c + k]
+        c_copy(c, src, g, k, MAIN, sem, parts=2).wait_recv()
 
     def d_rest(src):
         ended(down_all.at[src, pl.ds(0, (n_grp - 1) * d_half)], d_late.at[src])
@@ -990,9 +997,13 @@
             def _():
                 c_pass(c, mate, (MAIN,))
 
-            @pl.when(c > 1)
+            @pl.when((c > 1) & (c < own - 1))
             def _():
                 c_pass(c, facing, [OUT] + across)
+
+            @pl.when(c == own - 1)
+            def _():
+                c_pass(c, facing, (OUT,))
 
         with jax.named_scope("begin"):
             each(0, own, begin)
@@ -1016,10 +1027,17 @@
             feed(own)
 
     def feed(c):
-        @pl.when(c < n_col)
+        @pl.when(c < n_col - 1)
         def _():
             c_send_on(c, f, (MAIN,))
             c_pass(c, mate, (MAIN,))
+
+        @pl.when(c == n_col - 1)
+        def _():
+            c_pass(c, mate, (MAIN,), 2)
+            c_send_on(c, f, (MAIN,), 2)
+            for copy in straight_copies():
+                copy.start()
 
     each(0, pieces, norms_out)
 
@@ -1027,7 +1045,7 @@
         c = jnp.where(
             i < hosted - 1,
             own + i,
-            jnp.where(i == hosted - 1, 0, jnp.where(i == hosted, n_col - 1, i - hosted)),
+            jnp.where(i == hosted - 1, n_col - 1, i - hosted),
         )
         with jax.named_scope("rest"):
             c_rest(c)
@@ -1052,14 +1070,28 @@
 
     def slot(s):
         c = own + s // 2
-        src = jnp.where(s % 2 == 0, facing, beyond)
+        last = c == n_col - 1
+        src = jnp.where((s % 2 == 0) ^ last, facing, beyond)
 
         @pl.when(s % 2 == 0)
         def _():
             feed(c + 2)
 
         with jax.named_scope("slot"):
-            c_pass(c, src, across)
+
+            @pl.when(jnp.logical_not(last))
+            def _():
+                c_pass(c, src, across)
+
+            @pl.when(s == slots - 2)
+            def _():
+                c_pass(c, beyond, across, 2)
+                each(own - moved, own, lambda m: tail(m, mate))
+
+            @pl.when(s == slots - 1)
+            def _():
+                for k in range(2):
+                    c_pass_part(c, facing, k)
 
         when = s - (slots - 14)
 
@@ -1087,13 +1119,8 @@
                 m_rest(0)
                 m_rest(1)
 
-        @pl.when(s == slots - 1)
-        def _():
-            for d in range(1, n_grp):
-                moved_copy(d).start()
-
-        done = jnp.clip(when - 7, 0, hosted - 2)
-        more = jnp.where(when == 13, n_col, jnp.clip(when - 6, 0, hosted - 2))
+        done = jnp.clip(when - 8, 0, hosted - 2)
+        more = jnp.where(when == 13, n_col, jnp.clip(when - 7, 0, hosted - 2))
         each(done, more, serve)
 
     @pl.when(inner)
@@ -1106,10 +1133,11 @@
 
     @pl.when(outer)
     def _():
-        each(ahead, n_col, lambda c: c_send_on(c, f, (MAIN,)))
+        each(ahead, n_col - 1, lambda c: c_send_on(c, f, (MAIN,)))
+        c_send_on(n_col - 1, f, (MAIN,), 2)
         for share in others:
             each(own, n_col, lambda c: c_send_late(c, f, share))
-            each(0, own - 1, lambda c: c_send_late(c, f, share))
+            each(0, own - moved, lambda c: c_send_late(c, f, share))
 
         def pass_own(c):
             with jax.named_scope("pass_own"):
@@ -1161,9 +1189,10 @@
             d_sent(2, across)
             c_sent(n_col, 2, (MAIN,))
             c_sent(own, 3, (OUT,))
-            c_sent(n_col, 2, across)
-            for d in range(1, n_grp):
-                moved_copy(d).wait_send()
+            c_sent(n_col - 1, 2, across)
+            c_sent(moved, 1, [TAIL + d for d in range(1, n_grp)])
+            for copy in straight_copies():
+                copy.wait_send()
             m_drain(1)
             ended(back, b_send.at[0])
 
@@ -1171,10 +1200,10 @@
         def _():
             ended(down_all.at[f], d_send.at[MAIN])
             c_sent(n_col, 1, (MAIN,))
-            late = n_col - 1
+            late = n_col - moved
             ended(
                 cols_all.at[pl.ds(0, late), 0, pl.ds(0, (n_grp - 1) * c_half)],
-                c_send.at[ACROSS + n_grp - 1],
+                c_send.at[LATE],
             )
             d_sent(3, across)
             c_sent(own, 3, across)
@@ -1195,12 +1224,12 @@
     own = n_col * 4 // 11
     pieces = 4
     ahead = n_col - 1
-    parts = 2
+    moved = 2
     vmem = pl.BlockSpec(memory_space=pltpu.VMEM)
     hbm = pl.BlockSpec(memory_space=pltpu.HBM)
     dma = pltpu.SemaphoreType.DMA
     return pl.pallas_call(
-        functools.partial(paired_kernel, (n_grp, n_fs, n_tp, sub, own, pieces, ahead, parts)),
+        functools.partial(paired_kernel, (n_grp, n_fs, n_tp, sub, own, pieces, ahead, moved)),
         out_shape=(
             jax.ShapeDtypeStruct((rows, model), jnp.bfloat16),
             jax.ShapeDtypeStruct((tokens, width), jnp.bfloat16),
@@ -1223,8 +1252,8 @@
             dma((1 + n_grp,)),
             dma((n_fs - 1, sub)),
             dma((n_fs,)),
-            dma((2 * n_grp,)),
-            dma((n_fs - 1, n_col * parts)),
+            dma((2 * n_grp + 2,)),
+            dma((n_fs - 1, n_col + 1)),
             dma((n_col,)),
             dma((2,)),
             dma((2,)),
@@ -1243,11 +1272,38 @@
     )(*(pltpu.with_memory_space_constraint(a, pltpu.HBM) for a in arguments))
 
 
+def write_kernel(mixed_ref, hidden_ref, mixed_out, hidden_out, sems):
+    copies = [
+        pltpu.make_async_copy(hidden_ref, hidden_out, sems.at[0]),
+        pltpu.make_async_copy(mixed_ref, mixed_out, sems.at[1]),
+    ]
+    for copy in copies:
+        copy.start()
+    for copy in copies:
+        copy.wait()
+
+
+def written(mixed, hidden):
+    return pl.pallas_call(
+        write_kernel,
+        out_shape=(
+            jax.ShapeDtypeStruct(mixed.shape, mixed.dtype),
+            jax.ShapeDtypeStruct(hidden.shape, hidden.dtype),
+        ),
+        in_specs=[pl.BlockSpec(memory_space=pltpu.VMEM)] * 2,
+        out_specs=(pl.BlockSpec(memory_space=pl.ANY),) * 2,
+        scratch_shapes=[pltpu.SemaphoreType.DMA((2,))],
+        compiler_params=pltpu.CompilerParams(vmem_limit_bytes=8 * 1024 * 1024),
+        name="write_out",
+    )(mixed, hidden)
+
+
 def fits_pairs(sizes, residual_in, down_weight, gate_weight):
     n_grp, n_fs, n_tp = sizes
     depth, width = gate_weight.shape
     return (
-        n_fs == 4
+        n_grp == 2
+        and n_fs == 4
         and n_tp % 2 == 0
         and width % 128 == 0
         and width // 128 >= 10
@@ -1279,7 +1335,7 @@
             gate_weight,
             up_weight,
         )
-        return paired_call(sizes, arguments)
+        return written(*paired_call(sizes, arguments))
     n_grp, n_fs, n_tp = sizes
     rows, model = residual_in.shape
     depth, width = gate_weight.shape

time: 114 us -> 111 us (0.974)
  local copies, waits for them, and re-layouts: 1.89 us -> 0 us
    pallas_call x1, Pallas kernels: 111 us -> 109 us  [paired_call(): pl.pallas_call(functools.partial(paired_kernel, (n_grp, n_fs, n_tp, sub,...]
    unnamed x2 -> x0, local copies, waits for them, and re-layouts: 1.89 us -> none
    pallas_call x0 -> x1, Pallas kernels: none -> 1.29 us  [written(): pl.pallas_call(write_kernel, out_shape=(jax.ShapeDtypeStruct(mixed.shape,...]
where the time goes in v4:
time: 111 us; the launch traced here: 110 us
  Pallas kernels  110 us (99%)
    pallas_call x1, Pallas kernels, paired_call(): pl.pallas_call(functools.partial(paired_kernel, (n_grp, n_fs, n_tp, sub,...  109 us

profile of v4, /device:TPU:0, one launch (start us, length us, event | category | flops | bytes accessed | tf_op | source)
XLA Modules:
  0.0 110.4 jit_solution(12817322011714261537)
XLA Ops:
  0.6 108.5 %paired_half_steps.1 = (bf16[128,2048]{1,0:T(8,128)(2,1)S(1)}, bf16[512,1408]{1,0:T(8,128)(2,1)S(1)}) custom-call(bf16[128,2048]{1,0:T(8,128)(2,1)} %res_ref.1, bf16[128,5632]{1,0:T(8,128)(2,1)} %hid_ref.1, bf16[1408,512]{1,0:T(8,128)(2,1)} %down_ref.1, bf16[128,2048]{1,0:T(8,128)(2,1)} %mix_ref.1, f32[2,2048]{1,0:T(2,128)} %gain_ref.1, ...), custom_call_target="tpu_custom_call" | custom-call | tf_op jit(solution)/shard_map/paired_half_steps/pallas_call | solution.py:1231
  109.1 1.3 %write_out.1 = (bf16[128,2048]{1,0:T(8,128)(2,1)}, bf16[512,1408]{1,0:T(8,128)(2,1)}) custom-call(bf16[128,2048]{1,0:T(8,128)(2,1)S(1)} %get-tuple-element.4.mixed_ref, bf16[512,1408]{1,0:T(8,128)(2,1)S(1)} %get-tuple-element.5.hidden_ref), custom_call_target="tpu_custom_call" | custom-call | tf_op jit(solution)/shard_map/write_out/pallas_call | solution.py:1287

commit v5 on v4

--- a/solution.py
+++ b/solution.py
@@ -555,6 +555,7 @@
     mix_now,
     gain_now,
     shift_now,
+    early,
     load_sem,
     d_send,
     d_recv,
@@ -593,6 +594,21 @@
     def own_rows(peer):
         return pl.ds(pl.multiple_of(peer * rows, rows), rows)
 
+    barrier = pltpu.get_barrier_semaphore()
+
+    def greet(device):
+        pl.semaphore_signal(barrier, inc=1, device_id=device, device_id_type=MESH)
+
+    for d in range(1, n_grp):
+        greet({"grp": lax.rem(g + d, n_grp)})
+    for d in range(1, n_tp):
+        greet({"tp": lax.rem(t + d, n_tp)})
+    greet({"fs": mate})
+
+    @pl.when(inner)
+    def _():
+        greet({"fs": facing})
+
     load_down = pltpu.make_async_copy(down_ref, down_all.at[f], load_sem.at[0])
     load_hid = pltpu.make_async_copy(hid_block(t), spread.at[own_rows(t)], load_sem.at[1])
 
@@ -634,21 +650,6 @@
         pltpu.make_async_copy(ref, ref, sem).wait()
 
     each(0, n_col, load_cols)
-
-    barrier = pltpu.get_barrier_semaphore()
-
-    def greet(device):
-        pl.semaphore_signal(barrier, inc=1, device_id=device, device_id_type=MESH)
-
-    for d in range(1, n_grp):
-        greet({"grp": lax.rem(g + d, n_grp)})
-    for d in range(1, n_tp):
-        greet({"tp": lax.rem(t + d, n_tp)})
-    greet({"fs": mate})
-
-    @pl.when(inner)
-    def _():
-        greet({"fs": facing})
 
     with jax.named_scope("barrier"):
         pl.semaphore_wait(barrier, n_grp - 1 + n_tp - 1 + 1 + inner.astype(jnp.int32))
@@ -707,7 +708,7 @@
         last = n_col - 1
         copies = []
         for share in others:
-            copies.append(c_copy(last, f, share, 0, MAIN, c_late.at[last], LATE))
+            copies.append(c_copy(last, f, share, 0, MAIN, c_late.at[n_col], LATE))
             copies.append(c_copy(own - 1, f, share, 0, MAIN, c_late.at[own - 1], LAST))
         return copies
 
@@ -728,10 +729,13 @@
     def d_send_late(src, share, j):
         d_copy(src, share, j, MAIN, d_late.at[src]).start()
 
+    def arrival(c, k, parts):
+        return c if parts == 1 else own + 2 * (c - own) + k
+
     def c_part_on(c, src, k, ways, parts):
         for way in ways:
             if way in (MAIN, OUT):
-                sem = c_recv.at[place_at(receiver_of(way), src), c + k]
+                sem = c_recv.at[place_at(receiver_of(way), src), arrival(c, k, parts)]
             else:
                 sem = c_late.at[c]
             c_copy(c, src, g, k, way, sem, parts=parts).start()
@@ -749,12 +753,12 @@
 
     def c_pass(c, src, ways, parts=1):
         for k in range(parts):
-            sem = c_recv.at[place_at(f, src), c + k]
+            sem = c_recv.at[place_at(f, src), arrival(c, k, parts)]
             c_copy(c, src, g, k, MAIN, sem, parts=parts).wait_recv()
             c_part_on(c, src, k, ways, parts)
 
     def c_pass_part(c, src, k):
-        sem = c_recv.at[place_at(f, src), c + k]
+        sem = c_recv.at[place_at(f, src), arrival(c, k, 2)]
         c_copy(c, src, g, k, MAIN, sem, parts=2).wait_recv()
 
     def d_rest(src):
@@ -919,7 +923,8 @@
 
     @pl.when(outer)
     def _():
-        each(0, ahead, lambda c: c_send_on(c, f, (MAIN,)))
+        each(0, own, lambda c: c_send_on(c, f, (MAIN,)))
+        each(own, ahead, lambda c: c_send_on(c, f, (MAIN,), 2))
 
     with jax.named_scope("first_pass"):
 
@@ -1029,8 +1034,8 @@
     def feed(c):
         @pl.when(c < n_col - 1)
         def _():
-            c_send_on(c, f, (MAIN,))
-            c_pass(c, mate, (MAIN,))
+            c_send_on(c, f, (MAIN,), 2)
+            c_pass(c, mate, (MAIN,), 2)
 
         @pl.when(c == n_col - 1)
         def _():
@@ -1047,22 +1052,49 @@
             own + i,
             jnp.where(i == hosted - 1, n_col - 1, i - hosted),
         )
-        with jax.named_scope("rest"):
-            c_rest(c)
-
-        @pl.when((c >= own) & (c < n_col - 1))
+        last = n_col - 1
+
+        @pl.when(c < last)
+        def _():
+            with jax.named_scope("rest"):
+                c_rest(c)
+
+        @pl.when((c >= own) & (c < last))
         def _():
             with jax.named_scope("prod1"):
                 back[c - own] = second_product(1, c)
             b_copy(c).start()
 
-        @pl.when(c == n_col - 1)
-        def _():
+        @pl.when(c == last)
+        def _():
+            def term(span, src):
+                here = pl.ds(pl.multiple_of(src * depth, depth), depth)
+                return jnp.dot(
+                    mixed_all[1, span, here],
+                    cols_all[last, src],
+                    preferred_element_type=jnp.float32,
+                )
+
+            def add(k):
+                src = jnp.where(k == 0, f, jnp.where(k == 1, mate, beyond))
+                early[...] += term(slice(None), src)
+
             def half(h):
                 span = tile_rows(h)
-                back[c - own, span] = second_product(1, c, span)
-                b_copy(c, span).start()
-
+                total = early[span] + term(span, facing)
+                gate = total[:, :lanes]
+                back[last - own, span] = (
+                    gate / (1.0 + jnp.exp(-gate)) * total[:, lanes:]
+                ).astype(jnp.bfloat16)
+                b_copy(last, span).start()
+
+            early[...] = jnp.zeros_like(early)
+            add(0)
+            with jax.named_scope("rest"):
+                ended(cols_all.at[last, pl.ds(0, 2), pl.ds(0, c_half)], c_late.at[last])
+            each(1, 3, add)
+            with jax.named_scope("rest_last"):
+                ended(cols_all.at[last, 0, pl.ds(0, c_half)], c_late.at[n_col])
             each(0, 2, half)
 
         with jax.named_scope("prod0"):
@@ -1081,17 +1113,17 @@
 
             @pl.when(jnp.logical_not(last))
             def _():
-                c_pass(c, src, across)
+                c_pass(c, src, across, 2)
 
             @pl.when(s == slots - 2)
             def _():
                 c_pass(c, beyond, across, 2)
-                each(own - moved, own, lambda m: tail(m, mate))
 
             @pl.when(s == slots - 1)
             def _():
                 for k in range(2):
                     c_pass_part(c, facing, k)
+                each(own - moved, own, lambda m: tail(m, mate))
 
         when = s - (slots - 14)
 
@@ -1133,7 +1165,7 @@
 
     @pl.when(outer)
     def _():
-        each(ahead, n_col - 1, lambda c: c_send_on(c, f, (MAIN,)))
+        each(ahead, n_col - 1, lambda c: c_send_on(c, f, (MAIN,), 2))
         c_send_on(n_col - 1, f, (MAIN,), 2)
         for share in others:
             each(own, n_col, lambda c: c_send_late(c, f, share))
@@ -1248,13 +1280,14 @@
             pltpu.VMEM((rows, model), jnp.bfloat16),
             pltpu.VMEM((2, model), jnp.float32),
             pltpu.VMEM((2, model), jnp.float32),
+            pltpu.VMEM((tokens, 2 * lanes), jnp.float32),
             dma((7,)),
             dma((1 + n_grp,)),
             dma((n_fs - 1, sub)),
             dma((n_fs,)),
             dma((2 * n_grp + 2,)),
-            dma((n_fs - 1, n_col + 1)),
-            dma((n_col,)),
+            dma((n_fs - 1, 2 * n_col - own)),
+            dma((n_col + 1,)),
             dma((2,)),
             dma((2,)),
             dma((2,)),

time: 111 us -> 111 us (level)
  no operation moved by 1% of the time
where the time goes in v5:
time: 111 us
  Pallas kernels  110 us (99%)
    pallas_call x1, Pallas kernels, paired_call(): pl.pallas_call(functools.partial(paired_kernel, (n_grp, n_fs, n_tp, sub,...  109 us

profile of v5, /device:TPU:0, one launch (start us, length us, event | category | flops | bytes accessed | tf_op | source)
XLA Modules:
  0.0 110.5 jit_solution(4053300037242347560)
XLA Ops:
  0.6 108.6 %paired_half_steps.1 = (bf16[128,2048]{1,0:T(8,128)(2,1)S(1)}, bf16[512,1408]{1,0:T(8,128)(2,1)S(1)}) custom-call(bf16[128,2048]{1,0:T(8,128)(2,1)} %res_ref.1, bf16[128,5632]{1,0:T(8,128)(2,1)} %hid_ref.1, bf16[1408,512]{1,0:T(8,128)(2,1)} %down_ref.1, bf16[128,2048]{1,0:T(8,128)(2,1)} %mix_ref.1, f32[2,2048]{1,0:T(2,128)} %gain_ref.1, ...), custom_call_target="tpu_custom_call" | custom-call | tf_op jit(solution)/shard_map/paired_half_steps/pallas_call | solution.py:1263
  109.2 1.3 %write_out.1 = (bf16[128,2048]{1,0:T(8,128)(2,1)}, bf16[512,1408]{1,0:T(8,128)(2,1)}) custom-call(bf16[128,2048]{1,0:T(8,128)(2,1)S(1)} %get-tuple-element.4.mixed_ref, bf16[512,1408]{1,0:T(8,128)(2,1)S(1)} %get-tuple-element.5.hidden_ref), custom_call_target="tpu_custom_call" | custom-call | tf_op jit(solution)/shard_map/write_out/pallas_call | solution.py:1320
